TPU v7x, 512 devices: a whole 4x4x16 slice. The times are simulated.
512 devices in a mesh: ep: 32 (over z, core), tp: 16 (over y, x).
Axes of the slice: x: 4, y: 4, z: 16, core: 2. Of those that a mesh axis runs over, the one named last changes fastest.
Arguments:
- query_rows: bfloat16 [16384, 2048], P('ep', 'tp'), may hold values from -6 to 6
- key_rows: bfloat16 [16384, 2048], P('ep', 'tp'), may hold values from -6 to 6
- value_rows: bfloat16 [16384, 4096], P('ep', 'tp'), may hold values from -6 to 6
- in_gate: float32 [16, 16384], P('tp', 'ep'), may hold values from -120 to 120
- forget_gate: float32 [16, 16384], P('tp', 'ep'), may hold values from -2 to 20
- out_gate: bfloat16 [16384, 4096], P('ep', 'tp'), may hold values from -6 to 6
- head_gain: float32 [4096], P('tp'), may hold values from 0.1 to 1.9
- mix_weight: bfloat16 [4096, 4096], P(None, 'tp'), may hold values from -0.09375 to 0.09375
- expert_input: bfloat16 [8192, 4096], P('ep', 'tp'), may hold values from -30 to 30
- routes: int32 [8192, 2], P('ep'), may hold values from 0 to 31, all different within a row; in each aligned block of 256 rows (0 to 255, 256 to 511, ...) at most 32 rows name the same one
- route_weight: float32 [8192, 2], P('ep'), may hold values from 0.25 to 1.25
- gate_weight: bfloat16 [32, 1024, 4096], P('ep', 'tp'), may hold values from -0.09375 to 0.09375
- up_weight: bfloat16 [32, 1024, 4096], P('ep', 'tp'), may hold values from -0.09375 to 0.09375
- down_weight: bfloat16 [32, 1024, 4096], P('ep', None, 'tp'), may hold values from -0.1875 to 0.1875
Outputs:
- mixer_out: bfloat16 [16384, 4096], P('ep', 'tp')
- expert_out: bfloat16 [8192, 4096], P('ep', 'tp')
Inputs may be any that keep to these rules, and one draw needn't show every extreme that they name: `routes`: each row names 2 different experts. In the rows of one device no expert is named by more than 32 rows, and in the rows of some device an expert is named by exactly 32 rows.
All inputs are finite; a program needn't handle non-finite values.
Results may differ from a plain program's by a relative error of at most 0.0057.
Values may be sent and summed in bfloat16 or wider, within the bound.
A program may use at most 128 MiB of HBM per device.

v0:
```python
import jax
import jax.numpy as jnp
from jax import lax
from jax.sharding import Mesh
from jax.sharding import PartitionSpec as P

D = 4096
BLOCK = 64
EP = ("ep_0", "ep_1")


EPSILON = 1e-06
LOG_FLOOR = -1e30
HIGHEST_PRECISION = lax.Precision.HIGHEST


def nothing_yet(x, identity):
    return jax.tree.map(
        lambda part, zero: jnp.zeros_like(part) + jnp.asarray(zero, part.dtype), x, identity
    )


def collected_together(x, axis):
    leaves = jax.tree.leaves(x)
    turns = sorted(range(len(leaves)), key=lambda k: -leaves[k].size)
    width = (1, *leaves[turns[0]].shape)[-1]
    lines = [
        jnp.pad(leaves[k].reshape(-1), (0, -leaves[k].size % width)).reshape(-1, width)
        for k in turns
    ]
    both, at, found = (lax.all_gather(jnp.concatenate(lines), axis), 0, {})
    for k, line in zip(turns, lines):
        share = both[:, at : at + len(line)].reshape(len(both), -1)
        found[k] = share[:, : leaves[k].size].reshape(-1, *leaves[k].shape)
        at += len(line)
    numbers = iter(range(len(leaves)))
    return jax.tree.map(lambda _: found[next(numbers)], x)


def prefix_by_axis(x, axes, combine, identity):
    before = start = nothing_yet(x, identity)
    subtotal = x
    for axis in reversed(axes):
        length, index = (lax.axis_size(axis), lax.axis_index(axis))
        pieces = collected_together(subtotal, axis)
        inside, subtotal = (start, start)
        for k in range(length):
            passed = k < index
            subtotal = combine(subtotal, jax.tree.map(lambda part: part[k], pieces))
            inside = jax.tree.map(lambda new, old: jnp.where(passed, new, old), subtotal, inside)
        before = combine(inside, before)
    return before


def joined_along(tiles, dim):
    dims = list(tiles.shape[1:])
    dims[dim] *= tiles.shape[0]
    return jnp.moveaxis(tiles, 0, dim).reshape(dims)


def copy_for_each(x, axis):
    copies = jnp.broadcast_to(x, (lax.axis_size(axis), *x.shape))
    return lax.all_to_all(copies, axis, split_axis=0, concat_axis=0, tiled=True)


def gather_directly(x, axis, dim):
    return joined_along(copy_for_each(x, axis), dim)


def combine(first_part, second_part):
    decay_first, max_first, memory_first, normal_first = first_part
    decay_second, max_second, memory_second, normal_second = second_part
    running_max = jnp.maximum(decay_second + max_first, max_second)
    keep_first = jnp.exp(decay_second + max_first - running_max)
    keep_second = jnp.exp(max_second - running_max)
    memory = (
        keep_first[..., None, None] * memory_first + keep_second[..., None, None] * memory_second
    )
    normalizer = keep_first[..., None] * normal_first + keep_second[..., None] * normal_second
    return (decay_first + decay_second, running_max, memory, normalizer)


def identity_state(head_count, key_width, value_width):
    return (
        jnp.zeros((head_count,), jnp.float32),
        jnp.full((head_count,), LOG_FLOOR, jnp.float32),
        jnp.zeros((head_count, key_width, value_width), jnp.float32),
        jnp.zeros((head_count, key_width), jnp.float32),
    )


def halfprod(form, left, right):
    return jnp.einsum(form, left, right, preferred_element_type=jnp.float32)


def prepare(query_heads, key_heads, value_heads, in_gate, forget_gate):
    head_count, length, key_width = query_heads.shape
    block_count = length // BLOCK
    query_blocks = query_heads.reshape(head_count, block_count, BLOCK, key_width)
    key_blocks = key_heads.reshape(head_count, block_count, BLOCK, key_width)
    value_blocks = value_heads.reshape(head_count, block_count, BLOCK, value_heads.shape[-1])
    log_input = in_gate.reshape(head_count, block_count, BLOCK)
    cumulative = jnp.cumsum(
        jax.nn.log_sigmoid(forget_gate).reshape(head_count, block_count, BLOCK), axis=-1
    )
    block_decay = cumulative[..., -1]
    weight_log = block_decay[..., None] - cumulative + log_input
    block_max = jnp.max(weight_log, axis=-1)
    weighted = (
        key_blocks.astype(jnp.float32) * jnp.exp(weight_log - block_max[..., None])[..., None]
    )
    normalizer = jnp.sum(weighted, axis=2)
    memory = halfprod("hcsk,hcsv->hckv", weighted.astype(jnp.bfloat16), value_blocks)
    return (
        (query_blocks, key_blocks, value_blocks, log_input, cumulative),
        (block_decay, block_max, memory, normalizer),
    )


def prefix(summary, initial):
    leading = jax.tree.map(lambda tensor: jnp.moveaxis(tensor, 1, 0), summary)

    def advance(running, current):
        return (combine(running, current), running)

    final_state, before = lax.scan(advance, initial, leading)
    return (final_state, jax.tree.map(lambda tensor: jnp.moveaxis(tensor, 0, 1), before))


def block_outputs(blocked, before):
    query_blocks, key_blocks, value_blocks, log_input, cumulative = blocked
    prior_max, prior_memory, prior_normal = (before[1], before[2], before[3])
    block_len = cumulative.shape[-1]
    scale = query_blocks.shape[-1] ** (-0.5)
    causal = jnp.tril(jnp.ones((block_len, block_len), dtype=bool))
    log_decay = jnp.where(
        causal,
        cumulative[..., :, None] - cumulative[..., None, :] + log_input[..., None, :],
        -jnp.inf,
    )
    log_inter = cumulative + prior_max[..., None]
    top_value = jnp.maximum(log_inter, jnp.max(log_decay, axis=-1))
    scores = (
        halfprod("hctk,hcsk->hcts", query_blocks, key_blocks)
        * scale
        * jnp.exp(log_decay - top_value[..., None])
    )
    carried = jnp.exp(log_inter - top_value) * scale
    query_wide = query_blocks.astype(jnp.float32)
    numerator = carried[..., None] * jnp.einsum(
        "hctk,hckv->hctv", query_wide, prior_memory, precision=HIGHEST_PRECISION
    ) + halfprod("hcts,hcsv->hctv", scores.astype(jnp.bfloat16), value_blocks)
    denominator = carried * jnp.einsum(
        "hctk,hck->hct", query_wide, prior_normal, precision=HIGHEST_PRECISION
    ) + jnp.sum(scores, axis=-1)
    return numerator / jnp.maximum(jnp.abs(denominator), jnp.exp(-top_value))[..., None]


def finish(head_values, out_gate, head_gain):
    head_count, block_count, block_len, value_width = head_values.shape
    per_head = jnp.transpose(head_values, (1, 2, 0, 3)).reshape(
        block_count * block_len, head_count, value_width
    )
    per_head = per_head * lax.rsqrt(jnp.mean(per_head * per_head, axis=-1, keepdims=True) + EPSILON)
    per_head = per_head.reshape(block_count * block_len, head_count * value_width) * head_gain
    per_head = per_head * jax.nn.sigmoid(out_gate.astype(jnp.float32))
    return per_head.astype(jnp.bfloat16)


def cell_heads(query_rows, key_rows, value_rows, in_gate, forget_gate, out_gate, head_gain):
    length = query_rows.shape[0]
    head_count = in_gate.shape[0]
    key_width = query_rows.shape[1] // head_count
    value_width = value_rows.shape[1] // head_count
    query_heads = query_rows.reshape(length, head_count, key_width).transpose(1, 0, 2)
    key_heads = key_rows.reshape(length, head_count, key_width).transpose(1, 0, 2)
    value_heads = value_rows.reshape(length, head_count, value_width).transpose(1, 0, 2)
    blocked, summary = prepare(query_heads, key_heads, value_heads, in_gate, forget_gate)
    initial = identity_state(head_count, key_width, value_width)
    final_state, before = prefix(summary, initial)
    incoming = prefix_by_axis(final_state, EP, combine, initial)
    expanded = jax.tree.map(lambda tensor: tensor[:, None], incoming)
    before = combine(expanded, before)
    return finish(block_outputs(blocked, before), out_gate, head_gain)


def body(
    query_rows,
    key_rows,
    value_rows,
    in_gate,
    forget_gate,
    out_gate,
    head_gain,
    mix_weight,
    expert_input,
    routes,
    route_weight,
    gate_weight,
    up_weight,
    down_weight,
):
    mixed_heads = cell_heads(
        query_rows, key_rows, value_rows, in_gate, forget_gate, out_gate, head_gain
    )
    gate_local = gate_weight[0]
    up_local = up_weight[0]
    down_local = down_weight[0]
    group_size = lax.axis_size(EP)
    token_count, fanout = routes.shape
    capacity = 2 * token_count * fanout // group_size
    slot_count = group_size * capacity
    chosen = routes.reshape(-1)
    one_hot = (chosen[:, None] == jnp.arange(group_size, dtype=jnp.int32)[None, :]).astype(
        jnp.int32
    )
    position = jnp.sum((jnp.cumsum(one_hot, axis=0) - one_hot) * one_hot, axis=1)
    target = chosen * capacity + position
    matches = (jnp.arange(slot_count, dtype=jnp.int32)[:, None] == target[None, :]).astype(
        jnp.int32
    )
    occupied = jnp.sum(matches, axis=1) > 0
    source_row = jnp.sum(
        matches * (jnp.arange(token_count * fanout, dtype=jnp.int32) // fanout)[None, :], axis=1
    )
    arrived = lax.all_to_all(
        jnp.where(
            occupied[:, None],
            jnp.take(expert_input, source_row, axis=0),
            jnp.zeros((), expert_input.dtype),
        ),
        EP,
        split_axis=0,
        concat_axis=0,
        tiled=True,
    )
    head_piece = lax.all_gather(mixed_heads, "tp", axis=1, tiled=True)
    token_piece = lax.all_gather(arrived, "tp", axis=1, tiled=True)
    mix_acc = jnp.dot(head_piece, mix_weight, preferred_element_type=jnp.float32)
    gate_acc = jnp.einsum("sd,fd->sf", token_piece, gate_local, preferred_element_type=jnp.float32)
    up_acc = jnp.einsum("sd,fd->sf", token_piece, up_local, preferred_element_type=jnp.float32)
    squares = jnp.sum(jnp.square(token_piece.astype(jnp.float32)), axis=1)
    mix_acc, gate_acc, up_acc, squares = (mix_acc, gate_acc, up_acc, squares)
    mixer_out = mix_acc.astype(jnp.bfloat16)
    inverse_rms = lax.rsqrt(squares / D + EPSILON)[:, None]
    hidden = (jax.nn.silu(gate_acc * inverse_rms) * (up_acc * inverse_rms)).astype(jnp.bfloat16)
    expert_rows = jnp.dot(
        gather_directly(hidden, "tp", 1), down_local, preferred_element_type=jnp.float32
    )
    returned_rows = lax.all_to_all(
        expert_rows.astype(jnp.bfloat16), EP, split_axis=0, concat_axis=0, tiled=True
    )
    picked_rows = (
        jnp.take(returned_rows, target, axis=0).reshape(token_count, fanout, -1).astype(jnp.float32)
    )
    expert_out = jnp.sum(picked_rows * route_weight[:, :, None], axis=1).astype(jnp.bfloat16)
    return (mixer_out, expert_out)


def solution(mesh):
    split = Mesh(mesh.devices.reshape(16, 2, mesh.shape["tp"]), ("ep_0", "ep_1", "tp"))
    in_specs = (
        P(EP, "tp"),
        P(EP, "tp"),
        P(EP, "tp"),
        P("tp", EP),
        P("tp", EP),
        P(EP, "tp"),
        P("tp"),
        P(None, "tp"),
        P(EP, "tp"),
        P(EP, None),
        P(EP, None),
        P(EP, "tp", None),
        P(EP, "tp", None),
        P(EP, None, "tp"),
    )
    out_specs = (P(EP, "tp"), P(EP, "tp"))
    return jax.shard_map(body, mesh=split, in_specs=in_specs, out_specs=out_specs, check_vma=False)
```

profile of v0, /device:TPU:1, one launch (start us, length us, event | category | flops | bytes accessed | tf_op | source)
XLA Modules:
  0.0 352.5 jit_solution(5622983685871281707)
XLA Ops:
  7.3 0.8 fusion.55
  8.6 0.5 broadcast.772
  9.1 1.3 reduce.22
  10.6 0.8 reshape.1181
  11.6 1.1 fusion.21
  12.6 1.5 convolution_bitcast_fusion
  14.2 36.5 %while.25 = (s32[]{:T(128)}, f32[1]{0:T(128)}, f32[1]{0:T(128)}, f32[1,128,256]{2,1,0:T(8,128)S(1)}, f32[1,128]{1,0:T(1,128)S(1)}, /*index=5*/f32[8,1]{0,1:T(1,1...) while((s32[]{:T(128)}, f32[1]{0:T(128)}, f32[1]{0:T(128)}, ...), condition=%wide.region_4.5_spmd.clone, body=%wide.region_3.4_spmd.clone.sunk | while | flops 164488 | bytes 659258 | solution.py:126
  14.2 0.6 constant_dynamic-slice_fusion.4
  16.7 0.7 bitcast_dynamic-update-slice_fusion.2
  17.4 0.6 constant_dynamic-update-slice_fusion.2
  18.7 0.6 constant_dynamic-slice_fusion.4
  21.2 0.7 bitcast_dynamic-update-slice_fusion.2
  21.9 0.6 constant_dynamic-update-slice_fusion.2
  23.2 0.6 constant_dynamic-slice_fusion.4
  25.7 0.7 bitcast_dynamic-update-slice_fusion.2
  26.5 0.6 constant_dynamic-update-slice_fusion.2
  27.8 0.6 constant_dynamic-slice_fusion.4
  30.3 0.7 bitcast_dynamic-update-slice_fusion.2
  31.1 0.6 constant_dynamic-update-slice_fusion.2
  32.4 0.6 constant_dynamic-slice_fusion.4
  34.9 0.7 bitcast_dynamic-update-slice_fusion.2
  35.7 0.6 constant_dynamic-update-slice_fusion.2
  37.0 0.6 constant_dynamic-slice_fusion.4
  39.5 0.7 bitcast_dynamic-update-slice_fusion.2
  40.2 0.5 constant_dynamic-update-slice_fusion.2
  41.5 0.6 constant_dynamic-slice_fusion.4
  44.0 0.7 bitcast_dynamic-update-slice_fusion.2
  44.7 0.5 constant_dynamic-update-slice_fusion.2
  46.0 0.6 constant_dynamic-slice_fusion.4
  48.5 0.7 bitcast_dynamic-update-slice_fusion.2
  49.2 0.6 constant_dynamic-update-slice_fusion.2
  50.7 0.5 copy-done.15
  51.2 8.5 %all-gather.2 = f32[2,131,256]{2,1,0:T(8,128)S(1)} all-gather(f32[1,131,256]{2,1,0:T(8,128)S(1)} %maximum_bitcast_fusion), channel_id=2, replica_groups=mesh['ep_0'=16,'ep_1'=2,'tp'=16] {'ep_1'}, dimensions={0}, use_global_device_ids=true | all-gather | bytes 402432 | tf_op jit(solution)/shard_map/all_gather | solution.py:31
  59.7 0.6 fusion.86
  60.3 0.5 fusion.87
  66.3 0.7 maximum_bitcast_fusion.1
  67.0 0.8 copy.54
  68.1 1.2 reduce-window.6
  69.7 0.6 convert_reduce_fusion
  70.5 3.9 %gather_fusion = bf16[1024,256]{1,0:T(8,128)(2,1)S(1)} fusion(bf16[256,256]{1,0:T(8,128)(2,1)S(1)} %copy-done.1, s32[1024]{0:T(1024)S(1)} %broadcast_clamp_fusion), kind=kCustom, calls=%fused_computation | custom fusion | bytes 1052672 | tf_op jit(solution)/shard_map/jit(_take)/gather | solution.py:229
  74.6 0.3 select_select_fusion
  74.9 48.4 %all_to_all.26 = bf16[32,32,256]{2,1,0:T(8,128)(2,1)} all-to-all(bf16[32,32,256]{2,1,0:T(8,128)(2,1)S(1)} %select_select_fusion), channel_id=1, replica_groups=mesh['ep_0'=16,'ep_1'=2,'tp'=16] {'ep_0','ep_1'}, dimensions={0} | all-to-all | bytes 1048576 | tf_op jit(solution)/shard_map/all_to_all | solution.py:226
  124.7 22.1 %all-gather.12.cloned.1.call-done = f32[16,131,256]{2,1,0:T(8,128)} async-done(((f32[1,131,256]{2,1,0:T(8,128)}), f32[16,131,256]{2,1,0:T(8,128)}) %all-gather.12.cloned.1.call-update) | async-done | bytes 2146320 | tf_op jit(solution)/shard_map/all_gather | solution.py:31
  146.8 1.1 fusion.82
  147.9 0.7 fusion.85
  149.2 0.6 fusion.84
  180.3 0.3 fusion.89
  181.0 2.0 fusion.26
  183.0 0.3 fusion.44
  183.3 0.8 multiply_reduce_fusion.2
  184.2 0.9 fusion.17
  185.1 59.3 %all-gather.10.cloned.1.call-done = bf16[1024,4096]{1,0:T(8,128)(2,1)} async-done(((bf16[1024,256]{1,0:T(8,128)(2,1)}), bf16[1024,4096]{1,0:T(8,128)(2,1)}) %all-gather.10.cloned.1.call-update) | async-done | bytes 8388624 | tf_op jit(solution)/shard_map/all_gather | solution.py:238
  244.4 5.2 %multiply_reduce_fusion = f32[1024]{0:T(1024)S(1)} fusion(bf16[1024,4096]{1,0:T(8,128)(2,1)} %all-gather.10.cloned.1.call-done), kind=kLoop, calls=%fused_computation.12 | loop fusion | flops 12581888 | bytes 8392704 | tf_op jit(solution)/shard_map/reduce_sum | solution.py:242
  249.6 0.5 copy-done.2
  250.1 2.7 convolution_multiply_fusion.3
  252.8 2.7 fusion.8
  255.8 35.5 %all_to_all.27 = bf16[16,1024,64]{1,2,0:T(8,128)(2,1)S(1)} all-to-all(bf16[16,1024,64]{1,2,0:T(8,128)(2,1)S(1)} %broadcast_in_dim.75), channel_id=1, replica_groups=mesh['ep_0'=16,'ep_1'=2,'tp'=16] {'tp'}, dimensions={0} | all-to-all | bytes 4194304 | tf_op jit(solution)/shard_map/all_to_all | solution.py:63
  291.3 1.6 convolution_convert_fusion
  292.9 15.3 %all-to-all-start.2 = ((bf16[32,32,256]{2,1,0:T(8,128)(2,1)}), bf16[32,32,256]{2,1,0:T(8,128)(2,1)S(1)}, u32[]{:S(2)}, u32[]{:S(2)}) async-start(bf16[32,32,256]{2,1,0:T(8,128)(2,1)} %bitcast.139), calls=%async_computation.2 | async-start | bytes 1048576 | tf_op jit(solution)/shard_map/all_to_all | solution.py:250
  309.1 22.7 %all-gather.8.cloned.1.call-done = bf16[512,4096]{1,0:T(8,128)(2,1)} async-done(((bf16[512,256]{1,0:T(8,128)(2,1)}), bf16[512,4096]{1,0:T(8,128)(2,1)}) %all-gather.8.cloned.1.call-update) | async-done | bytes 4194320 | tf_op jit(solution)/shard_map/all_gather | solution.py:237
  331.8 4.1 %convolution_convert_fusion.1 = bf16[512,256]{1,0:T(8,128)(2,1)} fusion(bf16[512,4096]{1,0:T(8,128)(2,1)} %all-gather.8.cloned.1.call-done, bf16[4096,256]{1,0:T(8,128)(2,1)S(1)} %copy-done), kind=kOutput, calls=%fused_computation.22 | convolution fusion | flops 1073872896 | bytes 6553600 | tf_op jit(solution)/shard_map/dot_general | solution.py:239
  335.9 5.8 %all-to-all-done.2 = bf16[32,32,256]{2,1,0:T(8,128)(2,1)S(1)} async-done(((bf16[32,32,256]{2,1,0:T(8,128)(2,1)}), bf16[32,32,256]{2,1,0:T(8,128)(2,1)S(1)}, u32[]{:S(2)}, u32[]{:S(2)}) %all-to-all-start.2) | async-done | bytes 524320 | tf_op jit(solution)/shard_map/all_to_all | solution.py:250
  341.7 1.9 gather_fusion.1
  343.8 2.2 multiply_reduce_fusion.1
  (150 shorter events, 6.6 us)
Async XLA Ops:
  7.2 324.6 %copy-start = (bf16[4096,256]{1,0:T(8,128)(2,1)S(1)}, bf16[4096,256]{1,0:T(8,128)(2,1)}, u32[]{:S(2)}) copy-start(bf16[4096,256]{1,0:T(8,128)(2,1)} %param.23) | copy-start | bytes 6291460
  7.2 139.6 %all-gather.12.cloned.1.call-start = ((), (), s32[]{:S(2)}) async-start(), calls=%async_computation.5 | async-start | bytes 2367488 | tf_op jit(solution)/shard_map/all_gather | solution.py:31
  8.4 5.7 %copy-start.7 = (f32[1,8,64]{2,1,0:T(8,128)}, f32[1,8,64]{2,1,0:T(8,128)S(1)}, u32[]{:S(2)}) copy-start(f32[1,8,64]{2,1,0:T(8,128)S(1)} %reduce_window_sum.28) | copy-start | bytes 6148
  11.3 2.8 copy-start.9
  14.1 56.4 %copy-start.1 = (bf16[256,256]{1,0:T(8,128)(2,1)S(1)}, bf16[256,256]{1,0:T(8,128)(2,1)}, u32[]{:S(2)}) copy-start(bf16[256,256]{1,0:T(8,128)(2,1)} %param.24) | copy-start | bytes 393220
  50.6 0.5 copy-start.15
  50.6 0.6 copy-start.17
  67.0 177.4 %all-gather.10.cloned.1.call-start = ((), (), s32[]{:S(2)}) async-start(), calls=%async_computation.4 | async-start | bytes 8912896 | tf_op jit(solution)/shard_map/all_gather | solution.py:238
  74.5 49.9 %copy-start.8 = (f32[1,8,64]{2,1,0:T(8,128)S(1)}, f32[1,8,64]{2,1,0:T(8,128)}, u32[]{:S(2)}) copy-start(f32[1,8,64]{2,1,0:T(8,128)} %copy-done.7) | copy-start | bytes 6148
  74.5 49.9 %copy-start.10 = (f32[8,64]{1,0:T(8,128)S(1)}, f32[8,64]{1,0:T(8,128)}, u32[]{:S(2)}) copy-start(f32[8,64]{1,0:T(8,128)} %copy-done.9) | copy-start | bytes 6148
  74.5 105.5 %copy-start.16 = (f32[8,1]{0,1:T(1,128)S(1)}, f32[8,1]{0,1:T(1,128)}, u32[]{:S(2)}) copy-start(f32[8,1]{0,1:T(1,128)} %copy-done.15) | copy-start | bytes 100
  74.5 105.5 %copy-start.18 = (f32[8,1]{0,1:T(1,128)S(1)}, f32[8,1]{0,1:T(1,128)}, u32[]{:S(2)}) copy-start(f32[8,1]{0,1:T(1,128)} %copy-done.17) | copy-start | bytes 100
  74.5 105.7 %copy-start.12 = (f32[8,1,128]{2,1,0:T(1,128)S(1)}, f32[8,1,128]{2,1,0:T(1,128)}, u32[]{:S(2)}) copy-start(f32[8,1,128]{2,1,0:T(1,128)} %get-tuple-element.83) | copy-start | bytes 12292
  74.5 105.8 %copy-start.22 = (bf16[512,128]{1,0:T(8,128)(2,1)S(1)}, bf16[512,128]{1,0:T(8,128)(2,1)}, u32[]{:S(2)}) copy-start(bf16[512,128]{1,0:T(8,128)(2,1)} %param.16) | copy-start | bytes 393220
  74.5 106.1 %copy-start.5 = (bf16[512,128]{1,0:T(8,128)(2,1)S(1)}, bf16[512,128]{1,0:T(8,128)(2,1)}, u32[]{:S(2)}) copy-start(bf16[512,128]{1,0:T(8,128)(2,1)} %param.17) | copy-start | bytes 393220
  123.3 59.7 %copy-start.3 = (bf16[512,256]{1,0:T(8,128)(2,1)S(1)}, bf16[512,256]{1,0:T(8,128)(2,1)}, u32[]{:S(2)}) copy-start(bf16[512,256]{1,0:T(8,128)(2,1)} %param.18) | copy-start | bytes 786436
  123.3 208.4 %all-gather.8.cloned.1.call-start = ((), (), s32[]{:S(2)}) async-start(), calls=%async_computation.3 | async-start | bytes 4456448 | tf_op jit(solution)/shard_map/all_gather | solution.py:237
  180.3 3.0 copy-start.19
  180.3 3.0 copy-start.23
  183.0 1.2 copy-start.6
  183.0 1.2 copy-start.14
  184.2 65.4 %copy-start.4 = (bf16[1,64,4096]{2,1,0:T(8,128)(2,1)S(1)}, bf16[1,64,4096]{2,1,0:T(8,128)(2,1)}, u32[]{:S(2)}) copy-start(bf16[1,64,4096]{2,1,0:T(8,128)(2,1)} %param.27) | copy-start | bytes 1572868
  244.4 5.8 %copy-start.2 = (bf16[1024,4096]{1,0:T(8,128)(2,1)S(1)}, bf16[1024,4096]{1,0:T(8,128)(2,1)}, u32[]{:S(2)}) copy-start(bf16[1024,4096]{1,0:T(8,128)(2,1)} %all-gather.10.cloned.1.call-done) | copy-start | bytes 25165828
  250.1 2.7 copy-start.20
  255.8 35.5 %copy-start.21 = (bf16[1,1024,256]{2,1,0:T(8,128)(2,1)S(1)}, bf16[1,1024,256]{2,1,0:T(8,128)(2,1)}, u32[]{:S(2)}) copy-start(bf16[1,1024,256]{2,1,0:T(8,128)(2,1)} %param.29) | copy-start | bytes 1572868
  291.3 17.0 %copy-start.11 = (s32[256,2]{0,1:T(2,128)S(1)}, s32[256,2]{0,1:T(2,128)}, u32[]{:S(2)}) copy-start(s32[256,2]{0,1:T(2,128)} %param.25) | copy-start | bytes 6148
  291.3 17.6 %copy-start.13 = (f32[256,2]{0,1:T(2,128)S(1)}, f32[256,2]{0,1:T(2,128)}, u32[]{:S(2)}) copy-start(f32[256,2]{0,1:T(2,128)} %param.26) | copy-start | bytes 6148
  292.9 48.8 %all-to-all-start.2 = ((bf16[32,32,256]{2,1,0:T(8,128)(2,1)}), bf16[32,32,256]{2,1,0:T(8,128)(2,1)S(1)}, u32[]{:S(2)}, u32[]{:S(2)}) async-start(bf16[32,32,256]{2,1,0:T(8,128)(2,1)} %bitcast.139), calls=%async_computation.2 | async-start | bytes 1048576 | tf_op jit(solution)/shard_map/all_to_all | solution.py:250
Sparse Core Ops, SparseCore 0:
  67.1 79.6 all-gather.11
  149.7 94.5 all-gather.9
  247.9 83.7 all-gather.7
where the time goes:
time: 354 us; the launch traced here: 352 us
  waiting for transfers between devices  110 us (31%)
  blocking collectives  92.4 us (26%)
  between operations  51.3 us (14%)
  other arithmetic  28 us (8%)
  local copies, waits for them, and re-layouts  21.4 us (6%)
  loops' own time  19.7 us (6%)
  starting transfers between devices  15.6 us (4%)
  matrix products  14.2 us (4%)
    all_gather x1, waiting for transfers between devices, body(): token_piece = lax.all_gather(arrived, 'tp', axis=1, tiled=True)  59.3 us
    all_to_all x1, blocking collectives, body(): lax.all_to_all(jnp.where(occupied[:, None], jnp.take(expert_input, source...  48.4 us
    all_to_all x1, blocking collectives, copy_for_each(): return lax.all_to_all(copies, axis, split_axis=0, concat_axis=0, tiled=True)  35.5 us
    all_gather x1, waiting for transfers between devices, body(): head_piece = lax.all_gather(mixed_heads, 'tp', axis=1, tiled=True)  22.7 us
    all_gather x1, waiting for transfers between devices, collected_together(): both, at, found = (lax.all_gather(jnp.concatenate(lines), axis), 0, {})  22.1 us
    another operation x1, loops' own time, prefix(): final_state, before = lax.scan(advance, initial, leading)  19.7 us
    all_to_all x1, starting transfers between devices, body(): lax.all_to_all(expert_rows.astype(jnp.bfloat16), EP, split_axis=0, concat...  15.3 us
    dynamic_update_slice x16, other arithmetic, prefix(): final_state, before = lax.scan(advance, initial, leading)  9.85 us
  transfers between devices with their start and end apart: 4, of which 4 were waited for; matrix products, arithmetic and copies ran while one was open for 9% of the time, Pallas kernels for 0%

commit v1 on v0

v1 whole, which is shorter than its diff:
```python
import functools

import jax
import jax.numpy as jnp
from jax import lax
from jax.experimental import pallas as pl
from jax.experimental.pallas import tpu as pltpu
from jax.sharding import PartitionSpec as P

MESH = pl.DeviceIdType.MESH
BF, F32 = jnp.bfloat16, jnp.float32
D = 4096
EPS = 1e-6
FLOOR = -1e30
NEG = -3e38
SCALE = 128**-0.5
HOPS = [8, 7, 9, 6, 10, 5, 11, 4, 12, 3, 13, 2, 14, 1, 15, 0]
NT = (((1,), (1,)), ((), ()))
TN = (((0,), (0,)), ((), ()))


def mm(a, b):
    return jnp.dot(a, b, preferred_element_type=F32)


def dg(a, b, dims):
    return lax.dot_general(a, b, dims, preferred_element_type=F32)


def kernel(
    q_ref, k_ref, v_ref, ig_ref, fg_ref, og_ref, gain_ref, mixw_hbm, x_ref, routes_ref, rw_ref,
    gate_hbm, up_hbm, down_hbm,
    out_a, out_b,
    mixw, downn, downt, wt, xs, xa, gsend, grecv, hid, rows, ret, mixed,
    p1s, p1r, auxr, p2s, p2r, seen, sel0, sel1, num_ref, col_ref,
    loc_sem, own_sem, w_send, w_recv, p_send, p_recv, d_send, d_recv,
    xg_send, xg_recv, g_send, g_recv, ag_send, ag_recv, r_send, r_recv,
):
    e, t = lax.axis_index("ep"), lax.axis_index("tp")
    z, c = e // 2, e % 2
    y, x = t // 4, t % 4

    def along(axis, d):
        return (e, y * 4 + (x + d) % 4) if axis == "x" else (e, ((y + d) % 4) * 4 + x)

    def send(src, dst, ss, rs, dev):
        copy = pltpu.make_async_remote_copy(
            src_ref=src, dst_ref=dst, send_sem=ss, recv_sem=rs, device_id=dev, device_id_type=MESH
        )
        copy.start()
        sends.append(copy)
        return copy

    def bytes_of(ref, sem):
        pltpu.make_async_copy(ref, ref, sem).wait()

    sends = []
    live = {}

    barrier = pltpu.get_barrier_semaphore()

    def hello(k, _):
        pl.semaphore_signal(barrier, inc=1, device_id=((e + k) % 32, t), device_id_type=MESH)
        return 0

    lax.fori_loop(1, 32, hello, 0)
    for axis in "xy":
        for d in (1, 2, 3):
            pl.semaphore_signal(barrier, inc=1, device_id=along(axis, d), device_id_type=MESH)

    own_g = pltpu.make_async_copy(
        gate_hbm.at[:, pl.ds(pl.multiple_of(y * 1024, 1024), 1024)], wt.at[y, pl.ds(0, 64)], own_sem.at[0]
    )
    own_u = pltpu.make_async_copy(
        up_hbm.at[:, pl.ds(pl.multiple_of(y * 1024, 1024), 1024)], wt.at[y, pl.ds(64, 64)], own_sem.at[1]
    )
    own_g.start()
    own_u.start()
    load_mix = pltpu.make_async_copy(mixw_hbm, mixw, loc_sem.at[0])
    load_down = pltpu.make_async_copy(down_hbm, downn, loc_sem.at[1])
    load_mix.start()
    load_down.start()
    turned = []
    for b in range(16):
        copy = pltpu.make_async_copy(
            down_hbm.at[pl.ds(64 * ((b % 4) * 4 + b // 4), 64)], downt.at[pl.ds(64 * b, 64)], loc_sem.at[2 + b]
        )
        copy.start()
        turned.append(copy)

    f = fg_ref[...]
    log_f = jnp.minimum(f, 0.0) - jnp.log1p(jnp.exp(-jnp.abs(f)))
    si = lax.broadcasted_iota(jnp.int32, (128, 512), 1)
    ri = lax.broadcasted_iota(jnp.int32, (128, 512), 0)
    c_row = jnp.zeros((1, 512), F32)
    for b in range(4):
        ti = ri + 128 * b
        col_ref[128 * b : 128 * b + 128, 0:1] = jnp.sum(
            jnp.where(si <= ti, log_f, 0.0), axis=1, keepdims=True
        )
        f_col = jnp.sum(jnp.where(si == ti, log_f, 0.0), axis=1, keepdims=True)
        c_row = c_row + jnp.sum(jnp.where(ti <= si, f_col, 0.0), axis=0, keepdims=True)
    a_row = ig_ref[...] - c_row
    a_max = jnp.max(a_row, axis=1, keepdims=True)
    g_all = jnp.sum(log_f, axis=1, keepdims=True)
    mem = jnp.zeros((128, 256), F32)
    norm = jnp.zeros((1, 128), F32)
    for b in range(4):
        ti = ri + 128 * b
        col_ref[128 * b : 128 * b + 128, 1:2] = jnp.max(
            jnp.where(si <= ti, a_row, NEG), axis=1, keepdims=True
        )
        a_col = jnp.max(jnp.where(si == ti, a_row, NEG), axis=1, keepdims=True)
        kw = k_ref[128 * b : 128 * b + 128].astype(F32) * jnp.exp(a_col - a_max)
        norm = norm + jnp.sum(kw, axis=0, keepdims=True)
        mem = mem + dg(kw.astype(BF), v_ref[128 * b : 128 * b + 128], TN)
    for h in range(2):
        p1s[16 * h : 16 * h + 16] = mem[:, 128 * h : 128 * h + 128].reshape(16, 8, 128)
    aux = jnp.concatenate(
        [norm, jnp.broadcast_to(g_all, (1, 128)), jnp.broadcast_to(g_all + a_max, (1, 128)), jnp.zeros((1, 128), F32)],
        axis=0,
    )
    auxr[e] = aux
    p1r[e] = p1s[e]

    pl.semaphore_wait(barrier, 37)

    def first(k, _):
        to = (e + k) % 32
        for src, dst, n in ((p1s.at[to], p1r.at[e], 0), (auxr.at[e], auxr.at[e], 1)):
            pltpu.make_async_remote_copy(
                src_ref=src, dst_ref=dst, send_sem=p_send.at[n], recv_sem=p_recv.at[n],
                device_id=(to, t), device_id_type=MESH,
            ).start()
        return 0

    lax.fori_loop(1, 32, first, 0)
    w_in = []
    for d in (1, 2, 3):
        there = (y + d) % 4
        cols = pl.ds(pl.multiple_of(there * 1024, 1024), 1024)
        for n, (src, half) in enumerate(((gate_hbm, 0), (up_hbm, 64))):
            w_in.append(
                send(
                    src.at[:, cols], wt.at[y, pl.ds(half, 64)], w_send.at[2 * d - 2 + n], w_recv.at[2 * d - 2 + n],
                    along("y", d),
                )
            )

    ei = lax.broadcasted_iota(jnp.int32, (256, 128), 1)
    r0, r1 = routes_ref[:, 0:1], routes_ref[:, 1:2]
    hot0, hot1 = (ei == r0).astype(F32), (ei == r1).astype(F32)
    low = (
        lax.broadcasted_iota(jnp.int32, (256, 256), 1) < lax.broadcasted_iota(jnp.int32, (256, 256), 0)
    ).astype(F32).astype(BF)
    cum0 = mm(low, hot0.astype(BF))
    cum1 = mm(low, hot1.astype(BF)) + jnp.sum(hot0, axis=0, keepdims=True)
    s0 = r0.astype(F32) * 32.0 + jnp.sum(hot0 * cum0, axis=1, keepdims=True)
    s1 = r1.astype(F32) * 32.0 + jnp.sum(hot1 * cum1, axis=1, keepdims=True)
    slot = lax.broadcasted_iota(jnp.int32, (256, 1024), 1).astype(F32)
    sel0[...] = (slot == s0).astype(F32).astype(BF)
    sel1[...] = (slot == s1).astype(F32).astype(BF)
    for b in range(4):
        lanes = slice(256 * b, 256 * b + 256)
        both = sel0[:, lanes] + sel1[:, lanes]
        xs[8 * b : 8 * b + 8] = dg(both, x_ref[...], TN).astype(BF).reshape(8, 32, 256)
    own_rows = pl.ds(pl.multiple_of(192 + 32 * c, 32), 32)
    xa[3, x, own_rows, :] = xs[e]

    def dispatch(n):
        for i in range(4 * n, 4 * n + 4):
            at = pl.ds(pl.multiple_of(64 * (i - 4 * n) + 32 * c, 32), 32)
            for other in (1, 0) if i < 15 else (1,):
                to = ((z - HOPS[i] + 16) % 16) * 2 + (c + other) % 2
                pltpu.make_async_remote_copy(
                    src_ref=xs.at[to], dst_ref=xa.at[n, x, at], send_sem=d_send, recv_sem=d_recv.at[n],
                    device_id=(to, t), device_id_type=MESH,
                ).start()

    dispatch(0)
    dispatch(1)

    for b in range(4):
        ti = ri + 128 * b
        w = 128 * b + 128
        at = slice(128 * b, w)
        s = dg(q_ref[at], k_ref[:w], NT) * SCALE
        gate = jnp.exp(jnp.where(si <= ti, a_row, NEG)[:, :w] - col_ref[at, 1:2])
        s = s * gate
        col_ref[at, 2:3] = jnp.sum(s, axis=1, keepdims=True)
        num_ref[at] = mm(s.astype(BF), v_ref[:w])

    def scan_prior():
        bytes_of(p1r.at[pl.ds(0, 31)], p_recv.at[0])
        bytes_of(auxr.at[pl.ds(0, 31)], p_recv.at[1])

        m, n, cc = jnp.full((1, 128), FLOOR, F32), jnp.zeros((1, 128), F32), jnp.zeros((8, 128), F32)
        for k in range(32):
            p2s[k] = cc
            seen[k, 0:1], seen[k, 1:2] = m, n
            if k < 31:
                n2, g2, m2 = auxr[k, 0:1], auxr[k, 1:2], auxr[k, 2:3]
                top = jnp.maximum(g2 + m, m2)
                k1, k2 = jnp.exp(g2 + m - top), jnp.exp(m2 - top)
                m, cc, n = top, k1 * cc + k2 * p1r[k], k1 * n + k2 * n2
        live["pm"], live["pn"] = seen[e, 0:1], seen[e, 1:2]
        p2r[e] = p2s[e]

        def second(k, _):
            to = (e + k) % 32
            pltpu.make_async_remote_copy(
                src_ref=p2s.at[to], dst_ref=p2r.at[e], send_sem=p_send.at[2], recv_sem=p_recv.at[2],
                device_id=(to, t), device_id_type=MESH,
            ).start()
            return 0

        lax.fori_loop(1, 32, second, 0)

    def gather_steps(buf, order, n, cut):
        inner, outer = order
        ci, co = (x, y) if inner == "x" else (y, x)
        ss, rs = ag_send.at[n], ag_recv.at[n]

        def one():
            own = buf.at[co, ci]
            live["g", n] = [send(own, own, ss.at[j], rs.at[j], along(inner, d)) for j, d in enumerate((1, -1 + 4))]

        def two():
            for copy in live["g", n]:
                copy.wait_recv()
            out = []
            for j, d in enumerate((1, 3)):
                part = buf.at[co, (ci - d + 4) % 4, pl.ds(j * cut, cut)]
                out.append(send(part, part, ss.at[2 + j], rs.at[2 + j], along(inner, d)))
            live["g", n] = out

        def three():
            for copy in live["g", n]:
                copy.wait_recv()
            own = buf.at[co]
            live["g", n] = [send(own, own, ss.at[4 + j], rs.at[4 + j], along(outer, d)) for j, d in enumerate((1, 3))]

        def four():
            for copy in live["g", n]:
                copy.wait_recv()
            out = []
            for j, d in enumerate((1, 3)):
                part = buf.at[(co - d + 4) % 4, pl.ds(2 * j, 2)]
                out.append(send(part, part, ss.at[6 + j], rs.at[6 + j], along(outer, d)))
            live["g", n] = out

        def last():
            for copy in live["g", n]:
                copy.wait_recv()

        return one, two, three, four, last

    mix_steps = [gather_steps(mixed.at[h], "xy" if h == 0 else "yx", 4 + h, 128) for h in range(2)]
    hid_steps = [gather_steps(hid.at[n], "xy" if n % 2 == 0 else "yx", n, 32) for n in range(4)]

    def cell_out():
        bytes_of(p2r.at[pl.ds(0, 31)], p_recv.at[2])
        pm, pn = live["pm"][:, 0:1], live["pn"]
        parts = []
        for h in range(2):
            whole = p2r[16 * h : 16 * h + 16].reshape(128, 128)
            hi = whole.astype(BF)
            parts.append((hi, (whole - hi.astype(F32)).astype(BF)))
        for b in range(4):
            at = slice(128 * b, 128 * b + 128)
            qb = q_ref[at]
            c_col, amx, den = col_ref[at, 0:1], col_ref[at, 1:2], col_ref[at, 2:3]
            local, inter = c_col + amx, c_col + pm
            top = jnp.maximum(local, inter)
            f_local, f_inter = jnp.exp(local - top), jnp.exp(inter - top) * SCALE
            qc = jnp.concatenate([mm(qb, hi) + mm(qb, lo) for hi, lo in parts], axis=1)
            num = f_inter * qc + f_local * num_ref[at]
            den = f_inter * jnp.sum(qb.astype(F32) * pn, axis=1, keepdims=True) + f_local * den
            hv = num / jnp.maximum(jnp.abs(den), jnp.exp(-top))
            hv = hv * lax.rsqrt(jnp.mean(hv * hv, axis=1, keepdims=True) + EPS)
            hv = hv * gain_ref[...] * jax.nn.sigmoid(og_ref[at].astype(F32))
            o, i = (y, x) if b < 2 else (x, y)
            mixed[b // 2, o, i, 128 * (b % 2) : 128 * (b % 2) + 128, :] = hv.astype(BF)
        for steps in mix_steps:
            steps[0]()

    def mix_out(h):
        mix_steps[h][4]()
        if h == 0:
            load_mix.wait()
        acc = jnp.zeros((256, 256), F32)
        for o in range(4):
            for i in range(4):
                at = o * 4 + i if h == 0 else i * 4 + o
                acc = acc + mm(mixed[h, o, i], mixw[256 * at : 256 * at + 256])
        out_a[256 * h : 256 * h + 256] = acc.astype(BF)

    def arrive(n):
        k = 8 if n < 3 else 7
        landed = xa.at[n, x, pl.ds(0, 32 * k)]
        bytes_of(landed, d_recv.at[n])
        own = xa.at[n, x]
        live["x", n] = [
            send(own, own, xg_send.at[n, j], xg_recv.at[n, j], along("x", d)) for j, d in enumerate((1, 3))
        ]

    def relay(n):
        for copy in live["x", n]:
            copy.wait_recv()
        out = []
        for j, d in enumerate((1, 3)):
            part = xa.at[n, (x - d + 4) % 4, pl.ds(128 * j, 128)]
            out.append(send(part, part, xg_send.at[n, 2 + j], xg_recv.at[n, 2 + j], along("x", d)))
        live["x", n] = out

    def project(n):
        for copy in live["x", n]:
            copy.wait_recv()
        if n == 0:
            own_g.wait()
            own_u.wait()
            for copy in w_in:
                copy.wait_recv()
        acc = jnp.zeros((512, 256), F32)
        sq = jnp.zeros((16, 256), F32)
        ones = jnp.ones((16, 256), BF)
        for j in range(4):
            xx = xa[n, j]
            w = wt[:, :, 256 * j : 256 * j + 256].reshape(512, 256)
            acc = acc + dg(w, xx, NT)
            wide = xx.astype(F32)
            wide = wide * wide
            hi = wide.astype(BF)
            lo = (wide - hi.astype(F32)).astype(BF)
            sq = sq + dg(ones, hi, NT) + dg(ones, lo, NT)
        hi = sq.astype(BF).astype(F32)
        mid = (sq - hi).astype(BF).astype(F32)
        lo = sq - hi - mid
        row = lax.broadcasted_iota(jnp.int32, (16, 256), 0)
        sq = jnp.where(row == 0, hi, jnp.where(row == 1, mid, jnp.where(row == 2, lo, 0.0))).astype(BF)
        for j in range(4):
            gsend[n, j, 0:128, :] = acc[128 * j : 128 * j + 128].astype(BF)
            gsend[n, j, 128:144, :] = sq
        live["p", n] = [
            send(
                gsend.at[n, (y + d) % 4], grecv.at[n, y], g_send.at[n, d - 1], g_recv.at[n, d - 1], along("y", d)
            )
            for d in (1, 2, 3)
        ]

    def activate(n):
        for copy in live["p", n]:
            copy.wait_recv()
        total = gsend[n, y].astype(F32)
        for d in (1, 2, 3):
            total = total + grecv[n, (y + d) % 4].astype(F32)
        sq = jnp.sum(total[128:144], axis=0, keepdims=True)
        inv = lax.rsqrt(sq / D + EPS)
        g, u = total[0:64] * inv, total[64:128] * inv
        o, i = (y, x) if n % 2 == 0 else (x, y)
        hid[n, o, i] = (g * jax.nn.sigmoid(g) * u).astype(BF)
        hid_steps[n][0]()

    def finish(n):
        hid_steps[n][4]()
        if n == 0:
            load_down.wait()
            for copy in turned:
                copy.wait()
        down = downn if n % 2 == 0 else downt
        res = dg(hid[n].reshape(1024, 256), down[...], TN).astype(BF)
        rows[8 * n : 8 * n + 8] = res.reshape(8, 32, 256)
        for b in range(8):
            i, cs = 4 * n + b // 2, b % 2
            if i < 15:
                to = ((z + HOPS[i]) % 16) * 2 + cs
                pltpu.make_async_remote_copy(
                    src_ref=rows.at[8 * n + b], dst_ref=ret.at[e], send_sem=r_send, recv_sem=r_recv,
                    device_id=(to, t), device_id_type=MESH,
                ).start()
        if n == 3:
            pltpu.make_async_remote_copy(
                src_ref=rows.at[31 - c], dst_ref=ret.at[e], send_sem=r_send, recv_sem=r_recv,
                device_id=(z * 2 + 1 - c, t), device_id_type=MESH,
            ).start()
            ret[e] = rows[30 + c]

    def collect():
        bytes_of(ret.at[pl.ds(0, 31)], r_recv)
        back = ret[...].reshape(1024, 256)
        w0, w1 = rw_ref[:, 0:1], rw_ref[:, 1:2]
        out_b[...] = (mm(sel0[...], back) * w0 + mm(sel1[...], back) * w1).astype(BF)

    plan = [
        (0.0, scan_prior),
        (0.1, lambda: dispatch(2)),
        (0.2, lambda: dispatch(3)),
        (10.0, cell_out),
        (17.0, lambda: [s[1]() for s in mix_steps]),
        (21.0, lambda: [s[2]() for s in mix_steps]),
        (30.0, lambda: [s[3]() for s in mix_steps]),
        (44.0, lambda: mix_out(0)),
        (44.1, lambda: mix_out(1)),
        (100.0, collect),
    ]
    for n, base in enumerate((5.0, 13.0, 23.0, 29.0)):
        stages = [
            arrive, relay, project, activate,
            lambda n: hid_steps[n][1](), lambda n: hid_steps[n][2](), lambda n: hid_steps[n][3](), finish,
        ]
        for j, stage in enumerate(stages):
            plan.append((base + 3.0 * j, functools.partial(stage, n)))
    for _, work in sorted(plan, key=lambda p: p[0]):
        work()

    for copy in sends:
        copy.wait_send()
    bytes_of(p1s.at[pl.ds(0, 31)], p_send.at[0])
    bytes_of(auxr.at[pl.ds(0, 31)], p_send.at[1])
    bytes_of(p2s.at[pl.ds(0, 31)], p_send.at[2])
    bytes_of(xs.at[pl.ds(0, 31)], d_send)
    bytes_of(rows.at[pl.ds(0, 31)], r_send)


def body(q, k, v, ig, fg, og, gain, mixw, xin, routes, rw, gate, up, down):
    vm = pl.BlockSpec(memory_space=pltpu.VMEM)
    hbm = pl.BlockSpec(memory_space=pl.ANY)
    dma = pltpu.SemaphoreType.DMA
    out_a, out_b = pl.pallas_call(
        kernel,
        out_shape=(jax.ShapeDtypeStruct((512, 256), BF), jax.ShapeDtypeStruct((256, 256), BF)),
        in_specs=[vm] * 7 + [hbm] + [vm] * 3 + [hbm] * 3,
        out_specs=(vm, vm),
        scratch_shapes=[
            pltpu.VMEM((4096, 256), BF),
            pltpu.VMEM((1024, 256), BF),
            pltpu.VMEM((1024, 256), BF),
            pltpu.VMEM((4, 128, 1024), BF),
            pltpu.VMEM((32, 32, 256), BF),
            pltpu.VMEM((4, 4, 256, 256), BF),
            pltpu.VMEM((4, 4, 144, 256), BF),
            pltpu.VMEM((4, 4, 144, 256), BF),
            pltpu.VMEM((4, 4, 4, 64, 256), BF),
            pltpu.VMEM((32, 32, 256), BF),
            pltpu.VMEM((32, 32, 256), BF),
            pltpu.VMEM((2, 4, 4, 256, 256), BF),
            pltpu.VMEM((32, 8, 128), F32),
            pltpu.VMEM((32, 8, 128), F32),
            pltpu.VMEM((32, 4, 128), F32),
            pltpu.VMEM((32, 8, 128), F32),
            pltpu.VMEM((32, 8, 128), F32),
            pltpu.VMEM((32, 8, 128), F32),
            pltpu.VMEM((256, 1024), BF),
            pltpu.VMEM((256, 1024), BF),
            pltpu.VMEM((512, 256), F32),
            pltpu.VMEM((512, 128), F32),
            dma((18,)),
            dma((2,)),
            dma((6,)),
            dma((6,)),
            dma((3,)),
            dma((3,)),
            dma,
            dma((4,)),
            dma((4, 4)),
            dma((4, 4)),
            dma((4, 3)),
            dma((4, 3)),
            dma((6, 8)),
            dma((6, 8)),
            dma,
            dma,
        ],
        compiler_params=pltpu.CompilerParams(
            collective_id=0, has_side_effects=True, vmem_limit_bytes=56 * 1024 * 1024
        ),
    )(q, k, v, ig, fg, og, gain.reshape(1, 256), mixw, xin, routes, rw, gate[0], up[0], down[0])
    return out_a, out_b


def solution(mesh):
    in_specs = (
        P("ep", "tp"), P("ep", "tp"), P("ep", "tp"), P("tp", "ep"), P("tp", "ep"), P("ep", "tp"), P("tp"),
        P(None, "tp"), P("ep", "tp"), P("ep", None), P("ep", None), P("ep", "tp", None), P("ep", "tp", None),
        P("ep", None, "tp"),
    )
    return jax.shard_map(
        body, mesh=mesh, in_specs=in_specs, out_specs=(P("ep", "tp"), P("ep", "tp")), check_vma=False
    )
```

time: 354 us -> 147 us (0.42)
  Pallas kernels: 0 us -> 140 us
  waiting for transfers between devices: 110 us -> 0 us
  blocking collectives: 92.4 us -> 0 us
  between operations: 51.3 us -> 0.64 us
  other arithmetic: 28 us -> 0 us
  loops' own time: 19.7 us -> 0 us
  starting transfers between devices: 15.6 us -> 0 us
  local copies, waits for them, and re-layouts: 21.4 us -> 6.19 us
  matrix products: 14.2 us -> 0 us
    pallas_call x0 -> x1, Pallas kernels: none -> 140 us  [body(): pl.pallas_call(kernel, out_shape=(jax.ShapeDtypeStruct((512, 256), BF), j...]
    all_gather x3 -> x0, waiting for transfers between devices: 104 us -> none  [the longest x1 59.3 us: body(): token_piece = lax.all_gather(arrived, 'tp', axis=1, tiled=True)]
    all_to_all x2 -> x0, blocking collectives: 83.9 us -> none  [the longest x1 48.4 us: body(): lax.all_to_all(jnp.where(occupied[:, None], jnp.take(expert_input, source...]
    another operation x1 -> x0, loops' own time: 19.7 us -> none  [prefix(): final_state, before = lax.scan(advance, initial, leading)]
    all_to_all x1 -> x0, starting transfers between devices: 15.3 us -> none  [body(): lax.all_to_all(expert_rows.astype(jnp.bfloat16), EP, split_axis=0, concat...]
    dot_general x9 -> x0, matrix products: 14.2 us -> none  [the longest x1 4.14 us: body(): jnp.dot(head_piece, mix_weight, preferred_element_type=jnp.float32)]
    dynamic_update_slice x16 -> x0, other arithmetic: 9.85 us -> none  [prefix(): final_state, before = lax.scan(advance, initial, leading)]
    reduce_sum x5 -> x0, other arithmetic: 9.17 us -> none  [the longest x1 5.22 us: body(): squares = jnp.sum(jnp.square(token_piece.astype(jnp.float32)), axis=1)]
  transfers between devices with their start and end apart: 4 -> 0, of which waited for: 4 -> 0; matrix products, arithmetic and copies ran while one was open for 9% -> 0% of each run, Pallas kernels for 0% -> 0%
where the time goes in v1:
time: 147 us; the launch traced here: 146 us
  Pallas kernels  140 us (95%)
  local copies, waits for them, and re-layouts  6.19 us (4%)
    pallas_call x1, Pallas kernels, body(): pl.pallas_call(kernel, out_shape=(jax.ShapeDtypeStruct((512, 256), BF), j...  140 us
    unnamed x4, local copies, waits for them, and re-layouts  6.19 us

profile of v1, /device:TPU:1, one launch (start us, length us, event | category | flops | bytes accessed | tf_op | source)
XLA Modules:
  0.0 146.4 jit_solution(5753150036161995991)
XLA Ops:
  0.6 1.5 %copy.16.routes_ref = s32[256,2]{1,0:T(8,128)} copy(s32[256,2]{0,1:T(2,128)} %param.23) | data formatting | bytes 4096 | tf_op args[9]
  2.1 1.5 %copy.17.rw_ref = f32[256,2]{1,0:T(8,128)} copy(f32[256,2]{0,1:T(2,128)} %param.24) | data formatting | bytes 4096 | tf_op args[10]
  3.6 139.6 %shard_map.149 = (bf16[512,256]{1,0:T(8,128)(2,1)}, bf16[256,256]{1,0:T(8,128)(2,1)}) custom-call(bf16[512,128]{1,0:T(8,128)(2,1)} %q_ref.1, bf16[512,128]{1,0:T(8,128)(2,1)} %k_ref.1, bf16[512,256]{1,0:T(8,128)(2,1)} %v_ref.1, f32[1,512]{1,0:T(1,128)} %ig_ref.1, f32[1,512]{1,0:T(1,128)} %fg_ref.1, bf16[512,256]{1,0:T(8,128)(2,1)} %og_ref.1, ...), custom_call_target="tpu_custom_call" | custom-call | tf_op jit(solution)/shard_map/pallas_call | solution.py:429
  143.2 1.7 %copy.20 = bf16[512,256]{1,0:T(8,128)(2,1)} copy(bf16[512,256]{1,0:T(8,128)(2,1)} %get-tuple-element.4) | data formatting | bytes 524288
  144.9 1.6 %copy.21 = bf16[256,256]{1,0:T(8,128)(2,1)} copy(bf16[256,256]{1,0:T(8,128)(2,1)} %get-tuple-element.5) | data formatting | bytes 262144

commit v2 on v1

v2 whole, which is shorter than its diff:
```python
import functools

import jax
import jax.numpy as jnp
from jax import lax
from jax.experimental import pallas as pl
from jax.experimental.pallas import tpu as pltpu
from jax.sharding import PartitionSpec as P

MESH = pl.DeviceIdType.MESH
BF, F32 = jnp.bfloat16, jnp.float32
D = 4096
EPS = 1e-6
FLOOR = -1e30
NEG = -3e38
SCALE = 128**-0.5
NC = 8
PER = 16 // NC
S = 1024 // NC
HOPS = [8, 7, 9, 6, 10, 5, 11, 4, 12, 3, 13, 2, 14, 1, 15, 0]
ORDER = [
    (9, 0), (0, 0), (0, 1), (1, 0), (1, 1), (0, 2), (2, 0), (2, 1), (3, 0), (0, 3), (1, 2), (3, 1),
    (0, 4), (4, 0), (1, 3), (0, 5), (2, 2), (4, 1), (0, 6), (0, 7), (1, 4), (5, 0), (2, 3), (5, 1),
    (3, 2), (1, 5), (3, 3), (1, 6), (6, 1), (4, 2), (1, 7), (2, 4), (6, 0), (4, 3), (2, 5), (2, 6),
    (11, 0), (3, 4), (10, 0), (7, 1), (5, 2), (10, 1), (2, 7), (7, 0), (5, 3), (3, 5), (3, 6), (10, 2),
    (4, 4), (3, 7), (8, 0), (6, 3), (10, 3), (8, 1), (6, 2), (4, 5), (4, 6), (4, 7), (12, 0), (7, 2),
    (5, 5), (5, 7), (5, 4), (7, 3), (5, 6), (6, 4), (8, 3), (13, 0), (6, 6), (8, 2), (6, 5), (6, 7),
    (7, 4), (7, 5), (14, 0), (8, 4), (8, 5), (7, 6), (7, 7), (8, 6), (15, 0), (8, 7), (16, 0),
]
NT = (((1,), (1,)), ((), ()))
TN = (((0,), (0,)), ((), ()))


def mm(a, b):
    return jnp.dot(a, b, preferred_element_type=F32)


def dg(a, b, dims):
    return lax.dot_general(a, b, dims, preferred_element_type=F32)


def kernel(
    q_ref, k_ref, v_ref, ig_ref, fg_ref, og_ref, gain_ref, mixw_hbm, x_ref, routes_ref, rw_ref,
    gate_hbm, up_hbm, down_hbm,
    out_a, out_b,
    wm, wr, downn, downt, wt, xs, xa, gsend, grecv, gfar, ggot, gown, qown, hid, rows, ret, mixed, mfar, mgot, msend, mrecv, mown,
    p1s, p1r, auxr, p2s, p2r, seen, sel0, sel1, num_ref, col_ref,
    loc_sem, own_sem, w_send, w_recv, p_send, p_recv, d_send, d_recv,
    xg_send, xg_recv, mw_send, mw_recv, ma_send, ma_recv, mr_send, mr_recv, g_send, g_recv, ag_send, ag_recv, r_send, r_recv,
):
    e, t = lax.axis_index("ep"), lax.axis_index("tp")
    z, c = e // 2, e % 2
    y, x = t // 4, t % 4

    def along(axis, d):
        return (e, y * 4 + (x + d) % 4) if axis == "x" else (e, ((y + d) % 4) * 4 + x)

    def send(src, dst, ss, rs, dev):
        copy = pltpu.make_async_remote_copy(
            src_ref=src, dst_ref=dst, send_sem=ss, recv_sem=rs, device_id=dev, device_id_type=MESH
        )
        copy.start()
        sends.append(copy)
        return copy

    def bytes_of(ref, sem):
        pltpu.make_async_copy(ref, ref, sem).wait()

    sends = []
    live = {}

    def once(name):
        fresh = name not in live
        live[name] = True
        return fresh

    barrier = pltpu.get_barrier_semaphore()

    def hello(k, _):
        pl.semaphore_signal(barrier, inc=1, device_id=((e + k) % 32, t), device_id_type=MESH)
        return 0

    lax.fori_loop(1, 32, hello, 0)
    for axis in "xy":
        for d in (1, 2, 3):
            pl.semaphore_signal(barrier, inc=1, device_id=along(axis, d), device_id_type=MESH)

    own_g = pltpu.make_async_copy(
        gate_hbm.at[:, pl.ds(pl.multiple_of(y * 1024, 1024), 1024)], wt.at[y, pl.ds(0, 64)], own_sem.at[0]
    )
    own_u = pltpu.make_async_copy(
        up_hbm.at[:, pl.ds(pl.multiple_of(y * 1024, 1024), 1024)], wt.at[y, pl.ds(64, 64)], own_sem.at[1]
    )
    own_g.start()
    own_u.start()
    load_mix = pltpu.make_async_copy(mixw_hbm.at[:, x], wm.at[x], loc_sem.at[0])
    load_down = pltpu.make_async_copy(down_hbm, downn, loc_sem.at[1])
    load_mix.start()
    load_down.start()
    turned = []
    for b in range(16):
        copy = pltpu.make_async_copy(
            down_hbm.at[pl.ds(64 * ((b % 4) * 4 + b // 4), 64)], downt.at[pl.ds(64 * b, 64)], loc_sem.at[2 + b]
        )
        copy.start()
        turned.append(copy)


    ei = lax.broadcasted_iota(jnp.int32, (256, 128), 1)
    di = lax.broadcasted_iota(jnp.int32, (256, 256), 0) == lax.broadcasted_iota(jnp.int32, (256, 256), 1)

    def column(row):
        return jnp.sum(jnp.where(di, row, 0.0), axis=1, keepdims=True)

    r0, r1 = (column(routes_ref[j : j + 1].astype(F32)) for j in (0, 1))
    ei = ei.astype(F32)
    hot0, hot1 = (ei == r0).astype(F32), (ei == r1).astype(F32)
    low = (
        lax.broadcasted_iota(jnp.int32, (256, 256), 1) < lax.broadcasted_iota(jnp.int32, (256, 256), 0)
    ).astype(F32).astype(BF)
    cum0 = mm(low, hot0.astype(BF))
    cum1 = mm(low, hot1.astype(BF)) + jnp.sum(hot0, axis=0, keepdims=True)
    s0 = r0 * 32.0 + jnp.sum(hot0 * cum0, axis=1, keepdims=True)
    s1 = r1 * 32.0 + jnp.sum(hot1 * cum1, axis=1, keepdims=True)
    slot = lax.broadcasted_iota(jnp.int32, (256, 1024), 1).astype(F32)
    sel0[...] = (slot == s0).astype(F32).astype(BF)
    sel1[...] = (slot == s1).astype(F32).astype(BF)
    for b in range(4):
        lanes = slice(256 * b, 256 * b + 256)
        both = sel0[:, lanes] + sel1[:, lanes]
        xs[8 * b : 8 * b + 8] = dg(both, x_ref[...], TN).astype(BF).reshape(8, 32, 256)
    own_rows = pl.ds(pl.multiple_of(S - 64 + 32 * c, 32), 32)
    xa[NC - 1, x, own_rows, :] = xs[e]

    def dispatch(n):
        for i in range(PER * n, PER * n + PER):
            at = pl.ds(pl.multiple_of(64 * (i - PER * n) + 32 * c, 32), 32)
            for other in (1, 0) if i < 15 else (1,):
                to = ((z - HOPS[i] + 16) % 16) * 2 + (c + other) % 2
                pltpu.make_async_remote_copy(
                    src_ref=xs.at[to], dst_ref=xa.at[n, x, at], send_sem=d_send, recv_sem=d_recv.at[n],
                    device_id=(to, t), device_id_type=MESH,
                ).start()

    pl.semaphore_wait(barrier, 37)
    for n in range(NC):
        dispatch(n)
    w_in = []
    for d in (1, 2, 3):
        there = (y + d) % 4
        cols = pl.ds(pl.multiple_of(there * 1024, 1024), 1024)
        for n, (src, half) in enumerate(((gate_hbm, 0), (up_hbm, 64))):
            w_in.append(
                send(
                    src.at[:, cols], wt.at[y, pl.ds(half, 64)], w_send.at[2 * d - 2 + n], w_recv.at[2 * d - 2 + n],
                    along("y", d),
                )
            )
    far = [
        send(
            mixw_hbm.at[pl.ds(2 * j, 2), (x + 2) % 4], wr.at[j], mw_send.at[j], mw_recv.at[j], along("x", d)
        )
        for j, d in enumerate((1, 3))
    ]

    f = fg_ref[...]
    log_f = jnp.minimum(f, 0.0) - jnp.log1p(jnp.exp(-jnp.abs(f)))
    si = lax.broadcasted_iota(jnp.int32, (128, 512), 1)
    ri = lax.broadcasted_iota(jnp.int32, (128, 512), 0)
    c_row = jnp.zeros((1, 512), F32)
    for b in range(4):
        ti = ri + 128 * b
        col_ref[128 * b : 128 * b + 128, 0:1] = jnp.sum(
            jnp.where(si <= ti, log_f, 0.0), axis=1, keepdims=True
        )
        f_col = jnp.sum(jnp.where(si == ti, log_f, 0.0), axis=1, keepdims=True)
        c_row = c_row + jnp.sum(jnp.where(ti <= si, f_col, 0.0), axis=0, keepdims=True)
    a_row = ig_ref[...] - c_row
    a_max = jnp.max(a_row, axis=1, keepdims=True)
    g_all = jnp.sum(log_f, axis=1, keepdims=True)
    mem = jnp.zeros((128, 256), F32)
    norm = jnp.zeros((1, 128), F32)
    for b in range(4):
        ti = ri + 128 * b
        col_ref[128 * b : 128 * b + 128, 1:2] = jnp.max(
            jnp.where(si <= ti, a_row, NEG), axis=1, keepdims=True
        )
        a_col = jnp.max(jnp.where(si == ti, a_row, NEG), axis=1, keepdims=True)
        kw = k_ref[128 * b : 128 * b + 128].astype(F32) * jnp.exp(a_col - a_max)
        norm = norm + jnp.sum(kw, axis=0, keepdims=True)
        mem = mem + dg(kw.astype(BF), v_ref[128 * b : 128 * b + 128], TN)
    for h in range(2):
        p1s[16 * h : 16 * h + 16] = mem[:, 128 * h : 128 * h + 128].reshape(16, 8, 128).astype(BF)
    lane = lax.broadcasted_iota(jnp.int32, (1, 128), 1)
    auxr[e, 0:1] = norm
    auxr[e, 1:2] = jnp.where(lane < 64, g_all, g_all + a_max)
    p1r[e] = p1s[e]

    def first(k, _):
        to = (e + k) % 32
        for src, dst, n in ((p1s.at[to], p1r.at[e], 0), (auxr.at[e], auxr.at[e], 1)):
            pltpu.make_async_remote_copy(
                src_ref=src, dst_ref=dst, send_sem=p_send.at[n], recv_sem=p_recv.at[n],
                device_id=(to, t), device_id_type=MESH,
            ).start()
        return 0

    lax.fori_loop(1, 32, first, 0)

    for b in range(4):
        ti = ri + 128 * b
        w = 128 * b + 128
        at = slice(128 * b, w)
        s = dg(q_ref[at], k_ref[:w], NT) * SCALE
        gate = jnp.exp(jnp.where(si <= ti, a_row, NEG)[:, :w] - col_ref[at, 1:2])
        s = s * gate
        col_ref[at, 2:3] = jnp.sum(s, axis=1, keepdims=True)
        num_ref[at] = mm(s.astype(BF), v_ref[:w])

    m_in = []

    def pass_weights():
        for j, d in enumerate((1, 3)):
            far[j].wait_recv()
            m_in.append(
                send(
                    wr.at[j], wm.at[(x - d + 4) % 4, pl.ds(2 * j, 2)], mw_send.at[2 + j], mw_recv.at[2 + j],
                    along("x", d),
                )
            )

    def near_weights(p):
        for j, d in enumerate((1, 3)):
            at = 4 + 2 * p + j
            m_in.append(
                send(mixw_hbm.at[p, (x + d) % 4], wm.at[x, p], mw_send.at[at], mw_recv.at[at], along("x", d))
            )

    def scan_prior():
        bytes_of(p1r.at[pl.ds(0, 31)], p_recv.at[0])
        bytes_of(auxr.at[pl.ds(0, 31)], p_recv.at[1])

        m, n, cc = jnp.full((1, 128), FLOOR, F32), jnp.zeros((1, 128), F32), jnp.zeros((8, 128), F32)
        for k in range(32):
            p2s[k] = cc.astype(BF)
            seen[k, 0:1], seen[k, 1:2] = m, n
            if k < 31:
                n2, g2, m2 = auxr[k, 0:1], auxr[k, 1:2, 0:1], auxr[k, 1:2, 64:65]
                top = jnp.maximum(g2 + m, m2)
                k1, k2 = jnp.exp(g2 + m - top), jnp.exp(m2 - top)
                m, cc, n = top, k1 * cc + k2 * p1r[k].astype(F32), k1 * n + k2 * n2
        live["pm"], live["pn"] = seen[e, 0:1], seen[e, 1:2]
        p2r[e] = p2s[e]

        def second(k, _):
            to = (e + k) % 32
            pltpu.make_async_remote_copy(
                src_ref=p2s.at[to], dst_ref=p2r.at[e], send_sem=p_send.at[2], recv_sem=p_recv.at[2],
                device_id=(to, t), device_id_type=MESH,
            ).start()
            return 0

        lax.fori_loop(1, 32, second, 0)

    def gather_steps(buf, order, n, cut):
        inner, outer = order
        ci, co = (x, y) if inner == "x" else (y, x)
        ss, rs = ag_send.at[n], ag_recv.at[n]

        def one():
            own = buf.at[co, ci]
            live["g", n] = [send(own, own, ss.at[j], rs.at[j], along(inner, d)) for j, d in enumerate((1, -1 + 4))]

        def two():
            for copy in live["g", n]:
                copy.wait_recv()
            out = []
            for j, d in enumerate((1, 3)):
                part = buf.at[co, (ci - d + 4) % 4, pl.ds(j * cut, cut)]
                out.append(send(part, part, ss.at[2 + j], rs.at[2 + j], along(inner, d)))
            live["g", n] = out

        def three():
            for copy in live["g", n]:
                copy.wait_recv()
            own = buf.at[co]
            live["g", n] = [send(own, own, ss.at[4 + j], rs.at[4 + j], along(outer, d)) for j, d in enumerate((1, 3))]

        def four():
            for copy in live["g", n]:
                copy.wait_recv()
            out = []
            for j, d in enumerate((1, 3)):
                part = buf.at[(co - d + 4) % 4, pl.ds(2 * j, 2)]
                out.append(send(part, part, ss.at[6 + j], rs.at[6 + j], along(outer, d)))
            live["g", n] = out

        def last():
            for copy in live["g", n]:
                copy.wait_recv()

        return one, two, three, four, last

    hid_steps = [gather_steps(hid.at[n], "xy" if n % 2 == 0 else "yx", n, 32) for n in range(NC)]

    def cell_out():
        bytes_of(p2r.at[pl.ds(0, 31)], p_recv.at[2])
        pm, pn = live["pm"][:, 0:1], live["pn"]
        parts = []
        for h in range(2):
            parts.append(p2r[16 * h : 16 * h + 16].reshape(128, 128))
        for b in range(4):
            at = slice(128 * b, 128 * b + 128)
            qb = q_ref[at]
            c_col, amx, den = col_ref[at, 0:1], col_ref[at, 1:2], col_ref[at, 2:3]
            local, inter = c_col + amx, c_col + pm
            top = jnp.maximum(local, inter)
            f_local, f_inter = jnp.exp(local - top), jnp.exp(inter - top) * SCALE
            qc = jnp.concatenate([mm(qb, part) for part in parts], axis=1)
            num = f_inter * qc + f_local * num_ref[at]
            den = f_inter * jnp.sum(qb.astype(F32) * pn, axis=1, keepdims=True) + f_local * den
            hv = num / jnp.maximum(jnp.abs(den), jnp.exp(-top))
            hv = hv * lax.rsqrt(jnp.mean(hv * hv, axis=1, keepdims=True) + EPS)
            hv = hv * gain_ref[...] * jax.nn.sigmoid(og_ref[at].astype(F32))
            mixed[y, at, :] = hv.astype(BF)
        own = mixed.at[y]
        live["m"] = [send(own, own, ma_send.at[j], ma_recv.at[j], along("y", d)) for j, d in enumerate((1, 3))]

    def mix_relay():
        for copy in live["m"]:
            copy.wait_recv()
        out = []
        for j, d in enumerate((1, 3)):
            part = mixed.at[(y - d + 4) % 4, pl.ds(256 * j, 256)]
            out.append(send(part, part, ma_send.at[2 + j], ma_recv.at[2 + j], along("y", d)))
        live["m"] = out

    def mix_part():
        for copy in live["m"]:
            copy.wait_recv()
        load_mix.wait()
        for copy in m_in:
            copy.wait_recv()
        for d in (2, 1, 3, 0):
            there = (x + d) % 4
            acc = mm(mixed[0], wm[there, 0])
            for j in range(1, 4):
                acc = acc + mm(mixed[j], wm[there, j])
            if d == 2:
                mfar[...] = acc.astype(BF).reshape(2, 256, 256)
                live["m"] = [
                    send(mfar.at[j], mgot.at[j], mr_send.at[j], mr_recv.at[j], along("x", w))
                    for j, w in enumerate((1, 3))
                ]
            else:
                mown[d] = acc

    def mix_sum():
        for copy in live["m"]:
            copy.wait_recv()
        out = []
        for j, d in enumerate((1, 3)):
            half = slice(256 * j, 256 * j + 256)
            rest = slice(256 - 256 * j, 512 - 256 * j)
            msend[j, half] = (mown[d, half] + mgot[j].astype(F32)).astype(BF)
            msend[j, rest] = mown[d, rest].astype(BF)
            out.append(send(msend.at[j], mrecv.at[j], mr_send.at[2 + j], mr_recv.at[2 + j], along("x", d)))
        live["m"] = out

    def mix_out():
        for copy in live["m"]:
            copy.wait_recv()
        out_a[...] = (mown[0] + mrecv[0].astype(F32) + mrecv[1].astype(F32)).astype(BF)

    def arrive(n):
        k = 2 * PER if n < NC - 1 else 2 * PER - 1
        landed = xa.at[n, x, pl.ds(0, 32 * k)]
        bytes_of(landed, d_recv.at[n])
        own = xa.at[n, x]
        live["x", n] = [
            send(own, own, xg_send.at[n, j], xg_recv.at[n, j], along("x", d)) for j, d in enumerate((1, 3))
        ]

    def relay(n):
        for copy in live["x", n]:
            copy.wait_recv()
        out = []
        for j, d in enumerate((1, 3)):
            part = xa.at[n, (x - d + 4) % 4, pl.ds(S // 2 * j, S // 2)]
            out.append(send(part, part, xg_send.at[n, 2 + j], xg_recv.at[n, 2 + j], along("x", d)))
        live["x", n] = out

    def project(n):
        for copy in live["x", n]:
            copy.wait_recv()
        if once("wt"):
            own_g.wait()
            own_u.wait()
            for copy in w_in:
                copy.wait_recv()
        acc = jnp.zeros((512, S), F32)
        sq = jnp.zeros((16, S), F32)
        ones = jnp.ones((16, 256), BF)
        for j in range(4):
            xx = xa[n, j]
            w = wt[:, :, 256 * j : 256 * j + 256].reshape(512, 256)
            acc = acc + dg(w, xx, NT)
            wide = xx.astype(F32)
            wide = wide * wide
            hi = wide.astype(BF)
            lo = (wide - hi.astype(F32)).astype(BF)
            sq = sq + dg(ones, hi, NT) + dg(ones, lo, NT)
        gown[n] = acc.reshape(4, 128, S)
        qown[n] = sq
        gfar[n, 0:128] = gown[n, (y + 2) % 4].astype(BF)
        gfar[n, 128:144] = in_three(sq)
        live["p", n] = [
            send(
                gfar.at[n, pl.ds(64 * j, 64 + 16 * j)], ggot.at[n, pl.ds(64 * j, 64 + 16 * j)],
                g_send.at[n, j], g_recv.at[n, j], along("y", d),
            )
            for j, d in enumerate((1, 3))
        ]

    def in_three(sq):
        hi = sq.astype(BF).astype(F32)
        mid = (sq - hi).astype(BF).astype(F32)
        row = lax.broadcasted_iota(jnp.int32, (16, S), 0)
        parts = jnp.where(row == 0, hi, jnp.where(row == 1, mid, jnp.where(row == 2, sq - hi - mid, 0.0)))
        return parts.astype(BF)

    def partial_sum(n):
        for copy in live["p", n]:
            copy.wait_recv()
        sq = qown[n]
        gsend[n, 0, 0:64] = (gown[n, (y + 1) % 4, 0:64] + ggot[n, 0:64].astype(F32)).astype(BF)
        gsend[n, 0, 64:128] = gown[n, (y + 1) % 4, 64:128].astype(BF)
        gsend[n, 0, 128:144] = in_three(sq)
        gsend[n, 1, 0:64] = gown[n, (y + 3) % 4, 0:64].astype(BF)
        gsend[n, 1, 64:128] = (gown[n, (y + 3) % 4, 64:128] + ggot[n, 64:128].astype(F32)).astype(BF)
        gsend[n, 1, 128:144] = in_three(sq + jnp.sum(ggot[n, 128:144].astype(F32), axis=0, keepdims=True))
        live["p", n] = [
            send(gsend.at[n, j], grecv.at[n, j], g_send.at[n, 2 + j], g_recv.at[n, 2 + j], along("y", d))
            for j, d in enumerate((1, 3))
        ]

    def activate(n):
        for copy in live["p", n]:
            copy.wait_recv()
        total = gown[n, y] + grecv[n, 0, 0:128].astype(F32) + grecv[n, 1, 0:128].astype(F32)
        sq = qown[n, 0:1] + jnp.sum(
            grecv[n, 0, 128:144].astype(F32) + grecv[n, 1, 128:144].astype(F32), axis=0, keepdims=True
        )
        inv = lax.rsqrt(sq / D + EPS)
        g, u = total[0:64] * inv, total[64:128] * inv
        o, i = (y, x) if n % 2 == 0 else (x, y)
        hid[n, o, i] = (g * jax.nn.sigmoid(g) * u).astype(BF)
        hid_steps[n][0]()

    def finish(n):
        hid_steps[n][4]()
        if once("down"):
            load_down.wait()
            for copy in turned:
                copy.wait()
        down = downn if n % 2 == 0 else downt
        res = dg(hid[n].reshape(1024, S), down[...], TN).astype(BF)
        rows[2 * PER * n : 2 * PER * n + 2 * PER] = res.reshape(2 * PER, 32, 256)
        for b in range(2 * PER):
            i, cs = PER * n + b // 2, b % 2
            if i < 15:
                to = ((z + HOPS[i]) % 16) * 2 + cs
                pltpu.make_async_remote_copy(
                    src_ref=rows.at[2 * PER * n + b], dst_ref=ret.at[e], send_sem=r_send, recv_sem=r_recv,
                    device_id=(to, t), device_id_type=MESH,
                ).start()
        if n == NC - 1:
            pltpu.make_async_remote_copy(
                src_ref=rows.at[31 - c], dst_ref=ret.at[e], send_sem=r_send, recv_sem=r_recv,
                device_id=(z * 2 + 1 - c, t), device_id_type=MESH,
            ).start()
            ret[e] = rows[30 + c]

    def collect():
        bytes_of(ret.at[pl.ds(0, 31)], r_recv)
        back = ret[...].reshape(1024, 256)
        w0, w1 = column(rw_ref[0:1]), column(rw_ref[1:2])
        out_b[...] = (mm(sel0[...], back) * w0 + mm(sel1[...], back) * w1).astype(BF)

    stages = [
        arrive, relay, project, partial_sum, activate,
        lambda n: hid_steps[n][1](), lambda n: hid_steps[n][2](), lambda n: hid_steps[n][3](), finish,
        lambda n: pass_weights(), near_weights, lambda n: scan_prior(), lambda n: cell_out(),
        lambda n: mix_relay(), lambda n: mix_part(), lambda n: mix_sum(), lambda n: mix_out(),
    ]
    for which, n in ORDER:
        stages[which](n)
    collect()

    for copy in sends:
        copy.wait_send()
    bytes_of(p1s.at[pl.ds(0, 31)], p_send.at[0])
    bytes_of(auxr.at[pl.ds(0, 31)], p_send.at[1])
    bytes_of(p2s.at[pl.ds(0, 31)], p_send.at[2])
    bytes_of(xs.at[pl.ds(0, 31)], d_send)
    bytes_of(rows.at[pl.ds(0, 31)], r_send)


def body(q, k, v, ig, fg, og, gain, mixw, xin, routes, rw, gate, up, down):
    vm = pl.BlockSpec(memory_space=pltpu.VMEM)
    hbm = pl.BlockSpec(memory_space=pl.ANY)
    dma = pltpu.SemaphoreType.DMA
    out_a, out_b = pl.pallas_call(
        kernel,
        out_shape=(jax.ShapeDtypeStruct((512, 256), BF), jax.ShapeDtypeStruct((256, 256), BF)),
        in_specs=[vm] * 7 + [hbm] + [vm] * 3 + [hbm] * 3,
        out_specs=(vm, vm),
        scratch_shapes=[
            pltpu.VMEM((4, 4, 256, 256), BF),
            pltpu.VMEM((2, 2, 256, 256), BF),
            pltpu.VMEM((1024, 256), BF),
            pltpu.VMEM((1024, 256), BF),
            pltpu.VMEM((4, 128, 1024), BF),
            pltpu.VMEM((32, 32, 256), BF),
            pltpu.VMEM((NC, 4, S, 256), BF),
            pltpu.VMEM((NC, 2, 144, S), BF),
            pltpu.VMEM((NC, 2, 144, S), BF),
            pltpu.VMEM((NC, 144, S), BF),
            pltpu.VMEM((NC, 144, S), BF),
            pltpu.VMEM((NC, 4, 128, S), F32),
            pltpu.VMEM((NC, 16, S), F32),
            pltpu.VMEM((NC, 4, 4, 64, S), BF),
            pltpu.VMEM((32, 32, 256), BF),
            pltpu.VMEM((32, 32, 256), BF),
            pltpu.VMEM((4, 512, 256), BF),
            pltpu.VMEM((2, 256, 256), BF),
            pltpu.VMEM((2, 256, 256), BF),
            pltpu.VMEM((2, 512, 256), BF),
            pltpu.VMEM((2, 512, 256), BF),
            pltpu.VMEM((4, 512, 256), F32),
            pltpu.VMEM((32, 8, 128), BF),
            pltpu.VMEM((32, 8, 128), BF),
            pltpu.VMEM((32, 2, 128), F32),
            pltpu.VMEM((32, 8, 128), BF),
            pltpu.VMEM((32, 8, 128), BF),
            pltpu.VMEM((32, 8, 128), F32),
            pltpu.VMEM((256, 1024), BF),
            pltpu.VMEM((256, 1024), BF),
            pltpu.VMEM((512, 256), F32),
            pltpu.VMEM((512, 128), F32),
            dma((18,)),
            dma((2,)),
            dma((6,)),
            dma((6,)),
            dma((3,)),
            dma((3,)),
            dma,
            dma((NC,)),
            dma((NC, 4)),
            dma((NC, 4)),
            dma((12,)),
            dma((12,)),
            dma((4,)),
            dma((4,)),
            dma((4,)),
            dma((4,)),
            dma((NC, 4)),
            dma((NC, 4)),
            dma((NC, 8)),
            dma((NC, 8)),
            dma,
            dma,
        ],
        compiler_params=pltpu.CompilerParams(
            collective_id=0, has_side_effects=True, vmem_limit_bytes=56 * 1024 * 1024
        ),
    )(q, k, v, ig, fg, og, gain.reshape(1, 256), mixw.reshape(4, 4, 256, 256), xin, routes.T, rw.T, gate[0], up[0], down[0])
    return out_a, out_b


def solution(mesh):
    in_specs = (
        P("ep", "tp"), P("ep", "tp"), P("ep", "tp"), P("tp", "ep"), P("tp", "ep"), P("ep", "tp"), P("tp"),
        P(None, "tp"), P("ep", "tp"), P("ep", None), P("ep", None), P("ep", "tp", None), P("ep", "tp", None),
        P("ep", None, "tp"),
    )
    return jax.shard_map(
        body, mesh=mesh, in_specs=in_specs, out_specs=(P("ep", "tp"), P("ep", "tp")), check_vma=False
    )
```

time: 147 us -> 110 us (0.75)
  Pallas kernels: 140 us -> 106 us
  local copies, waits for them, and re-layouts: 6.19 us -> 3.24 us
    pallas_call x1, Pallas kernels: 140 us -> 106 us  [body(): pl.pallas_call(kernel, out_shape=(jax.ShapeDtypeStruct((512, 256), BF), j...]
    unnamed x4 -> x2, local copies, waits for them, and re-layouts: 6.19 us -> 3.24 us
where the time goes in v2:
time: 110 us
  Pallas kernels  106 us (96%)
  local copies, waits for them, and re-layouts  3.24 us (3%)
    pallas_call x1, Pallas kernels, body(): pl.pallas_call(kernel, out_shape=(jax.ShapeDtypeStruct((512, 256), BF), j...  106 us
    unnamed x2, local copies, waits for them, and re-layouts  3.24 us

profile of v2, /device:TPU:1, one launch (start us, length us, event | category | flops | bytes accessed | tf_op | source)
XLA Modules:
  0.0 110.2 jit_solution(12974247589669699015)
XLA Ops:
  0.6 106.3 %shard_map.149 = (bf16[512,256]{1,0:T(8,128)(2,1)}, bf16[256,256]{1,0:T(8,128)(2,1)}) custom-call(bf16[512,128]{1,0:T(8,128)(2,1)} %q_ref.1, bf16[512,128]{1,0:T(8,128)(2,1)} %k_ref.1, bf16[512,256]{1,0:T(8,128)(2,1)} %v_ref.1, f32[1,512]{1,0:T(1,128)} %ig_ref.1, f32[1,512]{1,0:T(1,128)} %fg_ref.1, bf16[512,256]{1,0:T(8,128)(2,1)} %og_ref.1, ...), custom_call_target="tpu_custom_call" | custom-call | tf_op jit(solution)/shard_map/pallas_call | solution.py:513
  107.0 1.7 %copy.18 = bf16[512,256]{1,0:T(8,128)(2,1)} copy(bf16[512,256]{1,0:T(8,128)(2,1)} %get-tuple-element.4) | data formatting | bytes 524288
  108.6 1.6 %copy.19 = bf16[256,256]{1,0:T(8,128)(2,1)} copy(bf16[256,256]{1,0:T(8,128)(2,1)} %get-tuple-element.5) | data formatting | bytes 262144

commit v3 on v2

v3 whole, which is shorter than its diff:
```python
import functools

import jax
import jax.numpy as jnp
from jax import lax
from jax.experimental import pallas as pl
from jax.experimental.pallas import tpu as pltpu
from jax.sharding import PartitionSpec as P

MESH = pl.DeviceIdType.MESH
BF, F32 = jnp.bfloat16, jnp.float32
D = 4096
EPS = 1e-6
FLOOR = -1e30
NEG = -3e38
SCALE = 128**-0.5
NC = 8
PER = 16 // NC
S = 1024 // NC
HOPS = [3, 13, 2, 14, 4, 12, 7, 9, 6, 10, 1, 15, 5, 11, 8, 0]
X_FIRST = [1, 0, 1, 0, 1, 1, 1, 0]
ORDER = [
    (17, 2), (18, 0), (17, 5), (17, 4), (19, 0), (17, 7), (10, 3), (0, 2), (10, 2), (17, 1), (17, 3), (0, 5),
    (17, 0), (0, 4), (1, 2), (1, 4), (1, 5), (0, 7), (2, 2), (0, 1), (17, 6), (2, 4), (3, 2), (1, 7),
    (20, 0), (3, 4), (1, 1), (2, 5), (0, 3), (0, 0), (2, 7), (4, 4), (4, 2), (1, 3), (3, 5), (0, 6),
    (3, 7), (5, 4), (5, 2), (1, 0), (2, 1), (2, 3), (4, 7), (6, 4), (1, 6), (9, 0), (6, 2), (11, 0),
    (3, 3), (4, 5), (5, 7), (3, 1), (7, 4), (2, 6), (2, 0), (6, 7), (4, 3), (7, 2), (10, 0), (8, 4),
    (4, 1), (3, 6), (3, 0), (5, 3), (12, 0), (7, 7), (4, 6), (5, 5), (4, 0), (8, 2), (5, 6), (8, 7),
    (5, 1), (6, 3), (10, 1), (6, 6), (7, 3), (13, 0), (6, 1), (6, 5), (5, 0), (7, 6), (8, 3), (7, 1),
    (6, 0), (14, 0), (7, 5), (8, 6), (7, 0), (15, 0), (8, 0), (8, 1), (8, 5), (16, 0),
]
NT = (((1,), (1,)), ((), ()))
TN = (((0,), (0,)), ((), ()))


def mm(a, b):
    return jnp.dot(a, b, preferred_element_type=F32)


def dg(a, b, dims):
    return lax.dot_general(a, b, dims, preferred_element_type=F32)


def kernel(
    q_hbm, k_hbm, v_hbm, ig_hbm, fg_hbm, og_hbm, gain_hbm, mixw_hbm, x_hbm, routes_hbm, rw_hbm,
    gate_hbm, up_hbm, down_hbm,
    far_a, far_b,
    q_ref, k_ref, v_ref, ig_ref, fg_ref, og_ref, gain_ref, x_ref, routes_ref, rw_ref, out_a, out_b,
    wm, wr, downn, downt, wt, xs, xa, gsend, grecv, gfar, ggot, gown, qown, hid, rows, ret, mixed, mfar, mgot, msend, mrecv, mown,
    p1s, p1r, p2s, p2r, seen, sel0, sel1, num_ref, col_ref,
    in_sem, out_sem, loc_sem, own_sem, w_send, w_recv, p_send, p_recv, d_send, d_recv,
    xg_send, xg_recv, far_send, far_recv, mw_send, mw_recv, ma_send, ma_recv, mr_send, mr_recv, g_send, g_recv,
    ag_near, ag_wide, ag_recv, r_send, r_recv,
):
    e, t = lax.axis_index("ep"), lax.axis_index("tp")
    z, c = e // 2, e % 2
    y, x = t // 4, t % 4

    def along(axis, d):
        return (e, y * 4 + (x + d) % 4) if axis == "x" else (e, ((y + d) % 4) * 4 + x)

    def send(src, dst, ss, rs, dev):
        copy = pltpu.make_async_remote_copy(
            src_ref=src, dst_ref=dst, send_sem=ss, recv_sem=rs, device_id=dev, device_id_type=MESH
        )
        copy.start()

    def bytes_of(ref, sem):
        pltpu.make_async_copy(ref, ref, sem).wait()

    live = {}

    def once(name):
        fresh = name not in live
        live[name] = True
        return fresh

    barrier = pltpu.get_barrier_semaphore()

    def hello(k, _):
        pl.semaphore_signal(barrier, inc=1, device_id=((e + k) % 32, t), device_id_type=MESH)
        return 0

    lax.fori_loop(1, 32, hello, 0)
    for axis in "xy":
        for d in (1, 2, 3):
            pl.semaphore_signal(barrier, inc=1, device_id=along(axis, d), device_id_type=MESH)

    arriving = []
    for j, (src, dst) in enumerate((
        (routes_hbm, routes_ref), (x_hbm, x_ref), (fg_hbm, fg_ref), (ig_hbm, ig_ref), (k_hbm, k_ref), (v_hbm, v_ref),
        (q_hbm, q_ref), (og_hbm, og_ref), (gain_hbm, gain_ref), (rw_hbm, rw_ref),
    )):
        copy = pltpu.make_async_copy(src, dst, in_sem.at[j])
        copy.start()
        arriving.append(copy)

    own_g = pltpu.make_async_copy(
        gate_hbm.at[:, pl.ds(pl.multiple_of(y * 1024, 1024), 1024)], wt.at[y, pl.ds(0, 64)], own_sem
    )
    own_u = pltpu.make_async_copy(
        up_hbm.at[:, pl.ds(pl.multiple_of(y * 1024, 1024), 1024)], wt.at[y, pl.ds(64, 64)], own_sem
    )
    own_g.start()
    own_u.start()
    load_mix = pltpu.make_async_copy(mixw_hbm.at[:, x], wm.at[x], loc_sem.at[0])
    load_down = pltpu.make_async_copy(down_hbm, downn, loc_sem.at[1])
    load_mix.start()
    load_down.start()
    turned = []
    for b in range(16 if not all(X_FIRST) else 0):
        copy = pltpu.make_async_copy(
            down_hbm.at[pl.ds(64 * ((b % 4) * 4 + b // 4), 64)], downt.at[pl.ds(64 * b, 64)], loc_sem.at[2]
        )
        copy.start()
        turned.append(copy)


    arriving[0].wait()
    ei = lax.broadcasted_iota(jnp.int32, (256, 128), 1)
    di = lax.broadcasted_iota(jnp.int32, (256, 256), 0) == lax.broadcasted_iota(jnp.int32, (256, 256), 1)

    def column(row):
        return jnp.sum(jnp.where(di, row, 0.0), axis=1, keepdims=True)

    r0, r1 = (column(routes_ref[j : j + 1].astype(F32)) for j in (0, 1))
    ei = ei.astype(F32)
    hot0, hot1 = (ei == r0).astype(F32), (ei == r1).astype(F32)
    low = (
        lax.broadcasted_iota(jnp.int32, (256, 256), 1) < lax.broadcasted_iota(jnp.int32, (256, 256), 0)
    ).astype(F32).astype(BF)
    cum0 = mm(low, hot0.astype(BF))
    cum1 = mm(low, hot1.astype(BF)) + jnp.sum(hot0, axis=0, keepdims=True)
    s0 = r0 * 32.0 + jnp.sum(hot0 * cum0, axis=1, keepdims=True)
    s1 = r1 * 32.0 + jnp.sum(hot1 * cum1, axis=1, keepdims=True)
    arriving[1].wait()
    slot = lax.broadcasted_iota(jnp.int32, (256, 1024), 1).astype(F32)
    sel0[...] = (slot == s0).astype(F32).astype(BF)
    sel1[...] = (slot == s1).astype(F32).astype(BF)
    for b in range(4):
        lanes = slice(256 * b, 256 * b + 256)
        both = sel0[:, lanes] + sel1[:, lanes]
        xs[8 * b : 8 * b + 8] = dg(both, x_ref[...], TN).astype(BF).reshape(8, 32, 256)
    own_rows = pl.ds(pl.multiple_of(S - 64 + 32 * c, 32), 32)
    xa[NC - 1, x, own_rows, :] = xs[e]

    def dispatch(n):
        for i in range(PER * n, PER * n + PER):
            at = pl.ds(pl.multiple_of(64 * (i - PER * n) + 32 * c, 32), 32)
            for other in (1, 0) if i < 15 else (1,):
                to = ((z - HOPS[i] + 16) % 16) * 2 + (c + other) % 2
                pltpu.make_async_remote_copy(
                    src_ref=xs.at[to], dst_ref=xa.at[n, x, at], send_sem=d_send, recv_sem=d_recv.at[n],
                    device_id=(to, t), device_id_type=MESH,
                ).start()

    pl.semaphore_wait(barrier, 37)
    def weights_out():
        for d in (1, 2, 3):
            cols = pl.ds(pl.multiple_of((y + d) % 4 * 1024, 1024), 1024)
            for src, half in ((gate_hbm, 0), (up_hbm, 64)):
                send(src.at[:, cols], wt.at[y, pl.ds(half, 64)], w_send, w_recv, along("y", d))

    def far_weights():
        for j, d in enumerate((1, 3)):
            send(mixw_hbm.at[pl.ds(2 * j, 2), (x + 2) % 4], wr.at[j], far_send, far_recv, along("x", d))

    si = lax.broadcasted_iota(jnp.int32, (128, 512), 1)
    ri = lax.broadcasted_iota(jnp.int32, (128, 512), 0)

    def states():
        for copy in arriving[2:6]:
            copy.wait()
        f = fg_ref[...]
        log_f = jnp.minimum(f, 0.0) - jnp.log1p(jnp.exp(-jnp.abs(f)))
        c_row = jnp.zeros((1, 512), F32)
        for b in range(4):
            ti = ri + 128 * b
            col_ref[128 * b : 128 * b + 128, 0:1] = jnp.sum(
                jnp.where(si <= ti, log_f, 0.0), axis=1, keepdims=True
            )
            f_col = jnp.sum(jnp.where(si == ti, log_f, 0.0), axis=1, keepdims=True)
            c_row = c_row + jnp.sum(jnp.where(ti <= si, f_col, 0.0), axis=0, keepdims=True)
        a_row = ig_ref[...] - c_row
        a_max = jnp.max(a_row, axis=1, keepdims=True)
        g_all = jnp.sum(log_f, axis=1, keepdims=True)
        mem = jnp.zeros((128, 256), F32)
        norm = jnp.zeros((1, 128), F32)
        for b in range(4):
            ti = ri + 128 * b
            col_ref[128 * b : 128 * b + 128, 1:2] = jnp.max(
                jnp.where(si <= ti, a_row, NEG), axis=1, keepdims=True
            )
            a_col = jnp.max(jnp.where(si == ti, a_row, NEG), axis=1, keepdims=True)
            kw = k_ref[128 * b : 128 * b + 128].astype(F32) * jnp.exp(a_col - a_max)
            norm = norm + jnp.sum(kw, axis=0, keepdims=True)
            mem = mem + dg(kw.astype(BF), v_ref[128 * b : 128 * b + 128], TN)
        lane = lax.broadcasted_iota(jnp.int32, (1, 128), 1)
        both = jnp.where(lane < 64, g_all, g_all + a_max)
        row = lax.broadcasted_iota(jnp.int32, (8, 128), 0)
        aux = jnp.zeros((8, 128), F32)
        for j, rest in enumerate((norm, both)):
            for n in range(3):
                part = rest.astype(BF).astype(F32)
                aux = jnp.where(row == 3 * j + n, part, aux)
                rest = rest - part
        for h in range(2):
            tiles = mem[:, 128 * h : 128 * h + 128].reshape(16, 8, 128)
            p1s[16 * h : 16 * h + 16] = jnp.concatenate(
                [tiles, jnp.broadcast_to(aux[None], (16, 8, 128))], axis=1
            ).astype(BF)
        p1r[e] = p1s[e]
        live["a_row"] = a_row

        def first(k, _):
            to = (e + k) % 32
            pltpu.make_async_remote_copy(
                src_ref=p1s.at[to], dst_ref=p1r.at[e], send_sem=p_send.at[0], recv_sem=p_recv.at[0],
                device_id=(to, t), device_id_type=MESH,
            ).start()
            return 0

        lax.fori_loop(1, 32, first, 0)

    def inside():
        a_row = live["a_row"]
        arriving[6].wait()
        for b in range(4):
            ti = ri + 128 * b
            w = 128 * b + 128
            at = slice(128 * b, w)
            s = dg(q_ref[at], k_ref[:w], NT) * SCALE
            gate = jnp.exp(jnp.where(si <= ti, a_row, NEG)[:, :w] - col_ref[at, 1:2])
            s = s * gate
            col_ref[at, 2:3] = jnp.sum(s, axis=1, keepdims=True)
            num_ref[at] = mm(s.astype(BF), v_ref[:w])

    def pass_weights():
        if "a_row" in live and once("inside"):
            inside()
        bytes_of(wr, far_recv)
        for j, d in enumerate((1, 3)):
            send(wr.at[j], wm.at[(x - d + 4) % 4, pl.ds(2 * j, 2)], mw_send, mw_recv, along("x", d))

    def near_weights(p):
        for d in (1, 3):
            send(mixw_hbm.at[p, (x + d) % 4], wm.at[x, p], mw_send, mw_recv, along("x", d))

    def scan_prior():
        if once("inside"):
            inside()
        bytes_of(p1r.at[pl.ds(0, 31)], p_recv.at[0])

        m, n, cc = jnp.full((1, 128), FLOOR, F32), jnp.zeros((1, 128), F32), jnp.zeros((8, 128), F32)
        for k in range(32):
            p2s[k] = cc.astype(BF)
            seen[k, 0:1], seen[k, 1:2] = m, n
            if k < 31:
                got = p1r[k].astype(F32)
                n2 = got[8:9] + got[9:10] + got[10:11]
                both = got[11:12] + got[12:13] + got[13:14]
                g2, m2 = both[:, 0:1], both[:, 64:65]
                top = jnp.maximum(g2 + m, m2)
                k1, k2 = jnp.exp(g2 + m - top), jnp.exp(m2 - top)
                m, cc, n = top, k1 * cc + k2 * got[0:8], k1 * n + k2 * n2
        live["pm"], live["pn"] = seen[e, 0:1], seen[e, 1:2]
        p2r[e] = p2s[e]

        def second(k, _):
            to = (e + k) % 32
            pltpu.make_async_remote_copy(
                src_ref=p2s.at[to], dst_ref=p2r.at[e], send_sem=p_send.at[1], recv_sem=p_recv.at[1],
                device_id=(to, t), device_id_type=MESH,
            ).start()
            return 0

        lax.fori_loop(1, 32, second, 0)

    def gather_steps(buf, order, n, cut):
        inner, outer = order
        ci, co = (x, y) if inner == "x" else (y, x)
        near, wide, rs = ag_near, ag_wide, ag_recv

        def one():
            own = buf.at[co, ci]
            for d in (1, 3):
                send(own, own, near, rs.at[n, 0], along(inner, d))

        def two():
            bytes_of(buf.at[co, pl.ds(0, 2)], rs.at[n, 0])
            for j, d in enumerate((1, 3)):
                part = buf.at[co, (ci - d + 4) % 4, pl.ds(j * cut, cut)]
                send(part, part, near, rs.at[n, 1], along(inner, d))

        def three():
            bytes_of(buf.at[co, 0], rs.at[n, 1])
            own = buf.at[co]
            for d in (1, 3):
                send(own, own, wide, rs.at[n, 2], along(outer, d))

        def four():
            bytes_of(buf.at[pl.ds(0, 2)], rs.at[n, 2])
            for j, d in enumerate((1, 3)):
                part = buf.at[(co - d + 4) % 4, pl.ds(2 * j, 2)]
                send(part, part, wide, rs.at[n, 3], along(outer, d))

        def last():
            bytes_of(buf.at[0], rs.at[n, 3])

        return one, two, three, four, last

    hid_steps = [gather_steps(hid.at[n], "xy" if X_FIRST[n] else "yx", n, 32) for n in range(NC)]

    def cell_out():
        for copy in arriving[7:9]:
            copy.wait()
        bytes_of(p2r.at[pl.ds(0, 31)], p_recv.at[1])
        pm, pn = live["pm"][:, 0:1], live["pn"]
        parts = []
        for h in range(2):
            parts.append(p2r[16 * h : 16 * h + 16].reshape(128, 128))
        for b in range(4):
            at = slice(128 * b, 128 * b + 128)
            qb = q_ref[at]
            c_col, amx, den = col_ref[at, 0:1], col_ref[at, 1:2], col_ref[at, 2:3]
            local, inter = c_col + amx, c_col + pm
            top = jnp.maximum(local, inter)
            f_local, f_inter = jnp.exp(local - top), jnp.exp(inter - top) * SCALE
            qc = jnp.concatenate([mm(qb, part) for part in parts], axis=1)
            num = f_inter * qc + f_local * num_ref[at]
            den = f_inter * jnp.sum(qb.astype(F32) * pn, axis=1, keepdims=True) + f_local * den
            hv = num / jnp.maximum(jnp.abs(den), jnp.exp(-top))
            hv = hv * lax.rsqrt(jnp.mean(hv * hv, axis=1, keepdims=True) + EPS)
            hv = hv * gain_ref[...] * jax.nn.sigmoid(og_ref[at].astype(F32))
            mixed[y, at, :] = hv.astype(BF)
        own = mixed.at[y]
        for d in (1, 3):
            send(own, own, ma_send, ma_recv.at[0], along("y", d))

    def mix_relay():
        bytes_of(mixed.at[pl.ds(0, 2)], ma_recv.at[0])
        for j, d in enumerate((1, 3)):
            part = mixed.at[(y - d + 4) % 4, pl.ds(256 * j, 256)]
            send(part, part, ma_send, ma_recv.at[1], along("y", d))

    def mix_part():
        bytes_of(mixed.at[0], ma_recv.at[1])
        load_mix.wait()
        bytes_of(wm.at[pl.ds(0, 3)], mw_recv)
        for d in (2, 1, 3, 0):
            there = (x + d) % 4
            acc = mm(mixed[0], wm[there, 0])
            for j in range(1, 4):
                acc = acc + mm(mixed[j], wm[there, j])
            if d == 2:
                mfar[...] = acc.astype(BF).reshape(2, 256, 256)
                for j, w in enumerate((1, 3)):
                    send(mfar.at[j], mgot.at[j], mr_send.at[0], mr_recv.at[0], along("x", w))
            else:
                mown[d] = acc

    def mix_sum():
        bytes_of(mgot, mr_recv.at[0])
        for j, d in enumerate((1, 3)):
            half = slice(256 * j, 256 * j + 256)
            rest = slice(256 - 256 * j, 512 - 256 * j)
            msend[j, half] = (mown[d, half] + mgot[j].astype(F32)).astype(BF)
            msend[j, rest] = mown[d, rest].astype(BF)
            send(msend.at[j], mrecv.at[j], mr_send.at[1], mr_recv.at[1], along("x", d))

    def mix_out():
        bytes_of(mrecv, mr_recv.at[1])
        out_a[...] = (mown[0] + mrecv[0].astype(F32) + mrecv[1].astype(F32)).astype(BF)
        pltpu.make_async_copy(out_a, far_a, out_sem.at[0]).start()

    def arrive(n):
        k = 2 * PER if n < NC - 1 else 2 * PER - 1
        landed = xa.at[n, x, pl.ds(0, 32 * k)]
        bytes_of(landed, d_recv.at[n])
        own = xa.at[n, x]
        for d in (1, 3):
            send(own, own, xg_send, xg_recv.at[n, 0], along("x", d))

    def relay(n):
        bytes_of(xa.at[n, pl.ds(0, 2)], xg_recv.at[n, 0])
        for j, d in enumerate((1, 3)):
            part = xa.at[n, (x - d + 4) % 4, pl.ds(S // 2 * j, S // 2)]
            send(part, part, xg_send, xg_recv.at[n, 1], along("x", d))

    def project(n):
        bytes_of(xa.at[n, 0], xg_recv.at[n, 1])
        if once("wt"):
            bytes_of(wt.at[y], own_sem)
            bytes_of(wt.at[pl.ds(0, 3)], w_recv)
        acc = jnp.zeros((512, S), F32)
        sq = jnp.zeros((16, S), F32)
        ones = jnp.ones((16, 256), BF)
        for j in range(4):
            xx = xa[n, j]
            w = wt[:, :, 256 * j : 256 * j + 256].reshape(512, 256)
            acc = acc + dg(w, xx, NT)
            wide = xx.astype(F32)
            wide = wide * wide
            hi = wide.astype(BF)
            lo = (wide - hi.astype(F32)).astype(BF)
            sq = sq + dg(ones, hi, NT) + dg(ones, lo, NT)
        gown[n] = acc.reshape(4, 128, S)
        qown[n] = sq
        gfar[n, 0:128] = gown[n, (y + 2) % 4].astype(BF)
        gfar[n, 128:144] = in_three(sq)
        for j, d in enumerate((1, 3)):
            at = pl.ds(64 * j, 64 + 16 * j)
            send(gfar.at[n, at], ggot.at[n, at], g_send.at[0], g_recv.at[n, 0], along("y", d))

    def in_three(sq):
        hi = sq.astype(BF).astype(F32)
        mid = (sq - hi).astype(BF).astype(F32)
        row = lax.broadcasted_iota(jnp.int32, (16, S), 0)
        parts = jnp.where(row == 0, hi, jnp.where(row == 1, mid, jnp.where(row == 2, sq - hi - mid, 0.0)))
        return parts.astype(BF)

    def partial_sum(n):
        bytes_of(ggot.at[n], g_recv.at[n, 0])
        sq = qown[n]
        gsend[n, 0, 0:64] = (gown[n, (y + 1) % 4, 0:64] + ggot[n, 0:64].astype(F32)).astype(BF)
        gsend[n, 0, 64:128] = gown[n, (y + 1) % 4, 64:128].astype(BF)
        gsend[n, 0, 128:144] = in_three(sq)
        gsend[n, 1, 0:64] = gown[n, (y + 3) % 4, 0:64].astype(BF)
        gsend[n, 1, 64:128] = (gown[n, (y + 3) % 4, 64:128] + ggot[n, 64:128].astype(F32)).astype(BF)
        gsend[n, 1, 128:144] = in_three(sq + jnp.sum(ggot[n, 128:144].astype(F32), axis=0, keepdims=True))
        for j, d in enumerate((1, 3)):
            send(gsend.at[n, j], grecv.at[n, j], g_send.at[1], g_recv.at[n, 1], along("y", d))

    def activate(n):
        bytes_of(grecv.at[n], g_recv.at[n, 1])
        total = gown[n, y] + grecv[n, 0, 0:128].astype(F32) + grecv[n, 1, 0:128].astype(F32)
        sq = qown[n, 0:1] + jnp.sum(
            grecv[n, 0, 128:144].astype(F32) + grecv[n, 1, 128:144].astype(F32), axis=0, keepdims=True
        )
        inv = lax.rsqrt(sq / D + EPS)
        g, u = total[0:64] * inv, total[64:128] * inv
        o, i = (y, x) if X_FIRST[n] else (x, y)
        hid[n, o, i] = (g * jax.nn.sigmoid(g) * u).astype(BF)
        hid_steps[n][0]()

    def finish(n):
        hid_steps[n][4]()
        if once("down"):
            load_down.wait()
            if turned:
                bytes_of(downt, loc_sem.at[2])
        down = downn if X_FIRST[n] else downt
        res = dg(hid[n].reshape(1024, S), down[...], TN).astype(BF)
        rows[2 * PER * n : 2 * PER * n + 2 * PER] = res.reshape(2 * PER, 32, 256)
        for b in range(2 * PER):
            i, cs = PER * n + b // 2, b % 2
            if i < 15:
                to = ((z + HOPS[i]) % 16) * 2 + cs
                pltpu.make_async_remote_copy(
                    src_ref=rows.at[2 * PER * n + b], dst_ref=ret.at[e], send_sem=r_send, recv_sem=r_recv,
                    device_id=(to, t), device_id_type=MESH,
                ).start()
        if n == NC - 1:
            pltpu.make_async_remote_copy(
                src_ref=rows.at[31 - c], dst_ref=ret.at[e], send_sem=r_send, recv_sem=r_recv,
                device_id=(z * 2 + 1 - c, t), device_id_type=MESH,
            ).start()
            ret[e] = rows[30 + c]

    def collect():
        arriving[9].wait()
        bytes_of(ret.at[pl.ds(0, 31)], r_recv)
        back = ret[...].reshape(1024, 256)
        w0, w1 = column(rw_ref[0:1]), column(rw_ref[1:2])
        out_b[...] = (mm(sel0[...], back) * w0 + mm(sel1[...], back) * w1).astype(BF)
        pltpu.make_async_copy(out_b, far_b, out_sem.at[1]).start()

    stages = [
        arrive, relay, project, partial_sum, activate,
        lambda n: hid_steps[n][1](), lambda n: hid_steps[n][2](), lambda n: hid_steps[n][3](), finish,
        lambda n: pass_weights(), near_weights, lambda n: scan_prior(), lambda n: cell_out(),
        lambda n: mix_relay(), lambda n: mix_part(), lambda n: mix_sum(), lambda n: mix_out(),
        dispatch, lambda n: far_weights(), lambda n: weights_out(), lambda n: states(),
    ]
    for which, n in ORDER:
        stages[which](n)
    collect()

    bytes_of(wt.at[pl.ds(0, 3)], w_send)
    bytes_of(wr, far_send)
    bytes_of(wm.at[pl.ds(0, 3)], mw_send)
    bytes_of(hid.at[:, 0, pl.ds(0, 3)], ag_near)
    bytes_of(hid.at[:, pl.ds(0, 3)], ag_wide)
    bytes_of(mixed.at[pl.ds(0, 3)], ma_send)
    bytes_of(mfar, mr_send.at[0])
    bytes_of(msend, mr_send.at[1])
    bytes_of(xa.at[:, pl.ds(0, 3)], xg_send)
    bytes_of(gfar, g_send.at[0])
    bytes_of(gsend, g_send.at[1])
    bytes_of(p1s.at[pl.ds(0, 31)], p_send.at[0])
    bytes_of(p2s.at[pl.ds(0, 31)], p_send.at[1])
    bytes_of(xs.at[pl.ds(0, 31)], d_send)
    bytes_of(rows.at[pl.ds(0, 31)], r_send)
    pltpu.make_async_copy(out_a, far_a, out_sem.at[0]).wait()
    pltpu.make_async_copy(out_b, far_b, out_sem.at[1]).wait()


def pass_on(a_in, b_in, a_out, b_out, a_mid, b_mid, sem):
    ins = [pltpu.make_async_copy(a_in, a_mid, sem.at[0]), pltpu.make_async_copy(b_in, b_mid, sem.at[1])]
    outs = [pltpu.make_async_copy(a_mid, a_out, sem.at[2]), pltpu.make_async_copy(b_mid, b_out, sem.at[3])]
    for copy in ins:
        copy.start()
    for copy, onward in zip(ins, outs):
        copy.wait()
        onward.start()
    for copy in outs:
        copy.wait()


def body(q, k, v, ig, fg, og, gain, mixw, xin, routes, rw, gate, up, down):
    hbm = pl.BlockSpec(memory_space=pl.ANY)
    dma = pltpu.SemaphoreType.DMA
    out_a, out_b = pl.pallas_call(
        kernel,
        out_shape=(jax.ShapeDtypeStruct((512, 256), BF), jax.ShapeDtypeStruct((256, 256), BF)),
        in_specs=[hbm] * 14,
        out_specs=(hbm, hbm),
        scratch_shapes=[
            pltpu.VMEM((512, 128), BF),
            pltpu.VMEM((512, 128), BF),
            pltpu.VMEM((512, 256), BF),
            pltpu.VMEM((1, 512), F32),
            pltpu.VMEM((1, 512), F32),
            pltpu.VMEM((512, 256), BF),
            pltpu.VMEM((1, 256), F32),
            pltpu.VMEM((256, 256), BF),
            pltpu.VMEM((2, 256), jnp.int32),
            pltpu.VMEM((2, 256), F32),
            pltpu.VMEM((512, 256), BF),
            pltpu.VMEM((256, 256), BF),
            pltpu.VMEM((4, 4, 256, 256), BF),
            pltpu.VMEM((2, 2, 256, 256), BF),
            pltpu.VMEM((1024, 256), BF),
            pltpu.VMEM((1024, 256), BF),
            pltpu.VMEM((4, 128, 1024), BF),
            pltpu.VMEM((32, 32, 256), BF),
            pltpu.VMEM((NC, 4, S, 256), BF),
            pltpu.VMEM((NC, 2, 144, S), BF),
            pltpu.VMEM((NC, 2, 144, S), BF),
            pltpu.VMEM((NC, 144, S), BF),
            pltpu.VMEM((NC, 144, S), BF),
            pltpu.VMEM((NC, 4, 128, S), F32),
            pltpu.VMEM((NC, 16, S), F32),
            pltpu.VMEM((NC, 4, 4, 64, S), BF),
            pltpu.VMEM((32, 32, 256), BF),
            pltpu.VMEM((32, 32, 256), BF),
            pltpu.VMEM((4, 512, 256), BF),
            pltpu.VMEM((2, 256, 256), BF),
            pltpu.VMEM((2, 256, 256), BF),
            pltpu.VMEM((2, 512, 256), BF),
            pltpu.VMEM((2, 512, 256), BF),
            pltpu.VMEM((4, 512, 256), F32),
            pltpu.VMEM((32, 16, 128), BF),
            pltpu.VMEM((32, 16, 128), BF),
            pltpu.VMEM((32, 8, 128), BF),
            pltpu.VMEM((32, 8, 128), BF),
            pltpu.VMEM((32, 8, 128), F32),
            pltpu.VMEM((256, 1024), BF),
            pltpu.VMEM((256, 1024), BF),
            pltpu.VMEM((512, 256), F32),
            pltpu.VMEM((512, 128), F32),
            dma((10,)),
            dma((2,)),
            dma((3,)),
            dma,
            dma,
            dma,
            dma((2,)),
            dma((2,)),
            dma,
            dma((NC,)),
            dma,
            dma((NC, 2)),
            dma,
            dma,
            dma,
            dma,
            dma,
            dma((2,)),
            dma((2,)),
            dma((2,)),
            dma((2,)),
            dma((NC, 2)),
            dma,
            dma,
            dma((NC, 4)),
            dma,
            dma,
        ],
        compiler_params=pltpu.CompilerParams(
            collective_id=0, has_side_effects=True, vmem_limit_bytes=56 * 1024 * 1024
        ),
    )(q, k, v, ig, fg, og, gain.reshape(1, 256), mixw.reshape(4, 4, 256, 256), xin, routes.T, rw.T, gate[0], up[0], down[0])
    return pl.pallas_call(
        pass_on,
        out_shape=(jax.ShapeDtypeStruct((512, 256), BF), jax.ShapeDtypeStruct((256, 256), BF)),
        in_specs=[hbm] * 2,
        out_specs=(hbm, hbm),
        scratch_shapes=[pltpu.VMEM((512, 256), BF), pltpu.VMEM((256, 256), BF), dma((4,))],
    )(out_a, out_b)


def solution(mesh):
    in_specs = (
        P("ep", "tp"), P("ep", "tp"), P("ep", "tp"), P("tp", "ep"), P("tp", "ep"), P("ep", "tp"), P("tp"),
        P(None, "tp"), P("ep", "tp"), P("ep", None), P("ep", None), P("ep", "tp", None), P("ep", "tp", None),
        P("ep", None, "tp"),
    )
    return jax.shard_map(
        body, mesh=mesh, in_specs=in_specs, out_specs=(P("ep", "tp"), P("ep", "tp")), check_vma=False
    )
```

time: 110 us -> 97.8 us (0.89)
  Pallas kernels: 106 us -> 97 us
  local copies, waits for them, and re-layouts: 3.24 us -> 0 us
    pallas_call x1, Pallas kernels: 106 us -> 95.2 us  [body(): pl.pallas_call(kernel, out_shape=(jax.ShapeDtypeStruct((512, 256), BF), j...]
    unnamed x2 -> x0, local copies, waits for them, and re-layouts: 3.24 us -> none
    pallas_call x0 -> x1, Pallas kernels: none -> 1.73 us  [body(): pl.pallas_call(pass_on, out_shape=(jax.ShapeDtypeStruct((512, 256), BF),...]
where the time goes in v3:
time: 97.8 us; the launch traced here: 97.6 us
  Pallas kernels  97 us (99%)
    pallas_call x1, Pallas kernels, body(): pl.pallas_call(kernel, out_shape=(jax.ShapeDtypeStruct((512, 256), BF), j...  95.2 us

profile of v3, /device:TPU:1, one launch (start us, length us, event | category | flops | bytes accessed | tf_op | source)
XLA Modules:
  0.0 97.6 jit_solution(9234254952272736762)
XLA Ops:
  0.6 95.2 %shard_map.149 = (bf16[512,256]{1,0:T(8,128)(2,1)}, bf16[256,256]{1,0:T(8,128)(2,1)}) custom-call(bf16[512,128]{1,0:T(8,128)(2,1)} %q_hbm.1, bf16[512,128]{1,0:T(8,128)(2,1)} %k_hbm.1, bf16[512,256]{1,0:T(8,128)(2,1)} %v_hbm.1, f32[1,512]{1,0:T(1,128)} %ig_hbm.1, f32[1,512]{1,0:T(1,128)} %fg_hbm.1, bf16[512,256]{1,0:T(8,128)(2,1)} %og_hbm.1, ...), custom_call_target="tpu_custom_call" | custom-call | tf_op jit(solution)/shard_map/pallas_call | solution.py:523
  95.9 1.7 %shard_map.150 = (bf16[512,256]{1,0:T(8,128)(2,1)}, bf16[256,256]{1,0:T(8,128)(2,1)}) custom-call(bf16[512,256]{1,0:T(8,128)(2,1)} %get-tuple-element.4.a_in, bf16[256,256]{1,0:T(8,128)(2,1)} %get-tuple-element.5.b_in), custom_call_target="tpu_custom_call" | custom-call | tf_op jit(solution)/shard_map/pallas_call | solution.py:604

commit v4 on v3

--- a/solution.py
+++ b/solution.py
@@ -17,17 +17,18 @@
 NC = 8
 PER = 16 // NC
 S = 1024 // NC
-HOPS = [3, 13, 2, 14, 4, 12, 7, 9, 6, 10, 1, 15, 5, 11, 8, 0]
-X_FIRST = [1, 0, 1, 0, 1, 1, 1, 0]
+HOPS = [7, 9, 6, 10, 5, 11, 4, 12, 3, 13, 2, 14, 1, 15, 8, 0]
+X_FIRST = [0, 1, 1, 0, 0, 0, 0, 0]
 ORDER = [
-    (17, 2), (18, 0), (17, 5), (17, 4), (19, 0), (17, 7), (10, 3), (0, 2), (10, 2), (17, 1), (17, 3), (0, 5),
-    (17, 0), (0, 4), (1, 2), (1, 4), (1, 5), (0, 7), (2, 2), (0, 1), (17, 6), (2, 4), (3, 2), (1, 7),
-    (20, 0), (3, 4), (1, 1), (2, 5), (0, 3), (0, 0), (2, 7), (4, 4), (4, 2), (1, 3), (3, 5), (0, 6),
-    (3, 7), (5, 4), (5, 2), (1, 0), (2, 1), (2, 3), (4, 7), (6, 4), (1, 6), (9, 0), (6, 2), (11, 0),
-    (3, 3), (4, 5), (5, 7), (3, 1), (7, 4), (2, 6), (2, 0), (6, 7), (4, 3), (7, 2), (10, 0), (8, 4),
-    (4, 1), (3, 6), (3, 0), (5, 3), (12, 0), (7, 7), (4, 6), (5, 5), (4, 0), (8, 2), (5, 6), (8, 7),
-    (5, 1), (6, 3), (10, 1), (6, 6), (7, 3), (13, 0), (6, 1), (6, 5), (5, 0), (7, 6), (8, 3), (7, 1),
-    (6, 0), (14, 0), (7, 5), (8, 6), (7, 0), (15, 0), (8, 0), (8, 1), (8, 5), (16, 0),
+    (10, 1), (17, 7), (10, 2), (17, 1), (19, 0), (21, 0), (17, 0), (17, 6), (17, 4), (18, 0), (10, 0), (0, 1),
+    (17, 3), (17, 5), (0, 7), (0, 6), (1, 1), (17, 2), (0, 0), (1, 7), (0, 4), (20, 0), (2, 1), (1, 0),
+    (0, 3), (2, 7), (1, 4), (0, 5), (3, 1), (2, 0), (3, 7), (1, 3), (4, 1), (0, 2), (2, 4), (3, 0),
+    (1, 6), (5, 1), (4, 7), (1, 5), (2, 3), (3, 4), (1, 2), (9, 0), (4, 0), (11, 0), (6, 1), (2, 6),
+    (2, 5), (5, 0), (4, 4), (5, 7), (3, 3), (2, 2), (7, 1), (3, 5), (6, 0), (3, 6), (5, 4), (4, 3),
+    (6, 7), (8, 1), (3, 2), (7, 0), (4, 6), (6, 4), (4, 5), (5, 3), (12, 0), (4, 2), (7, 7), (8, 0),
+    (5, 6), (6, 3), (5, 2), (7, 4), (5, 5), (8, 7), (10, 3), (7, 3), (13, 0), (6, 2), (8, 4), (6, 6),
+    (6, 5), (13, 1), (22, 0), (14, 0), (7, 2), (8, 3), (7, 6), (7, 5), (14, 1), (8, 2), (15, 0), (8, 5),
+    (15, 1), (8, 6), (16, 0), (16, 1),
 ]
 NT = (((1,), (1,)), ((), ()))
 TN = (((0,), (0,)), ((), ()))
@@ -46,11 +47,11 @@
     gate_hbm, up_hbm, down_hbm,
     far_a, far_b,
     q_ref, k_ref, v_ref, ig_ref, fg_ref, og_ref, gain_ref, x_ref, routes_ref, rw_ref, out_a, out_b,
-    wm, wr, downn, downt, wt, xs, xa, gsend, grecv, gfar, ggot, gown, qown, hid, rows, ret, mixed, mfar, mgot, msend, mrecv, mown,
+    dwait, rwait, wm, wr, downn, downt, wt, xs, xa, gsend, grecv, gfar, ggot, gown, qown, hid, rows, ret, mixed, mfar, mgot, msend, mrecv, mown,
     p1s, p1r, p2s, p2r, seen, sel0, sel1, num_ref, col_ref,
     in_sem, out_sem, loc_sem, own_sem, w_send, w_recv, p_send, p_recv, d_send, d_recv,
     xg_send, xg_recv, far_send, far_recv, mw_send, mw_recv, ma_send, ma_recv, mr_send, mr_recv, g_send, g_recv,
-    ag_near, ag_wide, ag_recv, r_send, r_recv,
+    ag_near, ag_wide, ag_recv, r_send, r_recv, t_send, t_recv,
 ):
     e, t = lax.axis_index("ep"), lax.axis_index("tp")
     z, c = e // 2, e % 2
@@ -149,6 +150,14 @@
             at = pl.ds(pl.multiple_of(64 * (i - PER * n) + 32 * c, 32), 32)
             for other in (1, 0) if i < 15 else (1,):
                 to = ((z - HOPS[i] + 16) % 16) * 2 + (c + other) % 2
+                if HOPS[i] == 8:
+                    to = ((z + 8) % 16) * 2 + 1 - other
+                if HOPS[i] == 8 and other == 0:
+                    pltpu.make_async_remote_copy(
+                        src_ref=xs.at[to], dst_ref=dwait, send_sem=d_send, recv_sem=t_recv.at[0],
+                        device_id=(((z + 15) % 16) * 2 + c, t), device_id_type=MESH,
+                    ).start()
+                    continue
                 pltpu.make_async_remote_copy(
                     src_ref=xs.at[to], dst_ref=xa.at[n, x, at], send_sem=d_send, recv_sem=d_recv.at[n],
                     device_id=(to, t), device_id_type=MESH,
@@ -246,6 +255,17 @@
         for d in (1, 3):
             send(mixw_hbm.at[p, (x + d) % 4], wm.at[x, p], mw_send, mw_recv, along("x", d))
 
+    at8 = HOPS.index(8)
+
+    def onward_rows():
+        bytes_of(dwait, t_recv.at[0])
+        at = pl.ds(pl.multiple_of(64 * (at8 % PER) + 32 * c, 32), 32)
+        send(dwait, xa.at[at8 // PER, x, at], t_send, d_recv.at[at8 // PER], (((z + 9) % 16) * 2 + 1, t))
+
+    def onward_results():
+        bytes_of(rwait, t_recv.at[1])
+        send(rwait, ret.at[(e + 2) % 32], t_send, r_recv, (((z + 9) % 16) * 2 + 1, t))
+
     def scan_prior():
         if once("inside"):
             inside()
@@ -332,46 +352,50 @@
             hv = num / jnp.maximum(jnp.abs(den), jnp.exp(-top))
             hv = hv * lax.rsqrt(jnp.mean(hv * hv, axis=1, keepdims=True) + EPS)
             hv = hv * gain_ref[...] * jax.nn.sigmoid(og_ref[at].astype(F32))
-            mixed[y, at, :] = hv.astype(BF)
-        own = mixed.at[y]
-        for d in (1, 3):
-            send(own, own, ma_send, ma_recv.at[0], along("y", d))
-
-    def mix_relay():
-        bytes_of(mixed.at[pl.ds(0, 2)], ma_recv.at[0])
+            h = b // 2
+            mixed[h, y, 128 * (b % 2) : 128 * (b % 2) + 128, :] = hv.astype(BF)
+            if b % 2:
+                own = mixed.at[h, y]
+                for d in (1, 3):
+                    send(own, own, ma_send, ma_recv.at[h, 0], along("y", d))
+
+    def mix_relay(h):
+        bytes_of(mixed.at[h, pl.ds(0, 2)], ma_recv.at[h, 0])
         for j, d in enumerate((1, 3)):
-            part = mixed.at[(y - d + 4) % 4, pl.ds(256 * j, 256)]
-            send(part, part, ma_send, ma_recv.at[1], along("y", d))
-
-    def mix_part():
-        bytes_of(mixed.at[0], ma_recv.at[1])
-        load_mix.wait()
-        bytes_of(wm.at[pl.ds(0, 3)], mw_recv)
+            part = mixed.at[h, (y - d + 4) % 4, pl.ds(128 * j, 128)]
+            send(part, part, ma_send, ma_recv.at[h, 1], along("y", d))
+
+    def mix_part(h):
+        bytes_of(mixed.at[h, 0], ma_recv.at[h, 1])
+        if once("wm"):
+            load_mix.wait()
+            bytes_of(wm.at[pl.ds(0, 3)], mw_recv)
         for d in (2, 1, 3, 0):
             there = (x + d) % 4
-            acc = mm(mixed[0], wm[there, 0])
+            acc = mm(mixed[h, 0], wm[there, 0])
             for j in range(1, 4):
-                acc = acc + mm(mixed[j], wm[there, j])
+                acc = acc + mm(mixed[h, j], wm[there, j])
             if d == 2:
-                mfar[...] = acc.astype(BF).reshape(2, 256, 256)
+                mfar[h] = acc.astype(BF).reshape(2, 128, 256)
                 for j, w in enumerate((1, 3)):
-                    send(mfar.at[j], mgot.at[j], mr_send.at[0], mr_recv.at[0], along("x", w))
+                    send(mfar.at[h, j], mgot.at[h, j], mr_send.at[0], mr_recv.at[h, 0], along("x", w))
             else:
-                mown[d] = acc
-
-    def mix_sum():
-        bytes_of(mgot, mr_recv.at[0])
+                mown[h, d] = acc
+
+    def mix_sum(h):
+        bytes_of(mgot.at[h], mr_recv.at[h, 0])
         for j, d in enumerate((1, 3)):
-            half = slice(256 * j, 256 * j + 256)
-            rest = slice(256 - 256 * j, 512 - 256 * j)
-            msend[j, half] = (mown[d, half] + mgot[j].astype(F32)).astype(BF)
-            msend[j, rest] = mown[d, rest].astype(BF)
-            send(msend.at[j], mrecv.at[j], mr_send.at[1], mr_recv.at[1], along("x", d))
-
-    def mix_out():
-        bytes_of(mrecv, mr_recv.at[1])
-        out_a[...] = (mown[0] + mrecv[0].astype(F32) + mrecv[1].astype(F32)).astype(BF)
-        pltpu.make_async_copy(out_a, far_a, out_sem.at[0]).start()
+            half = slice(128 * j, 128 * j + 128)
+            rest = slice(128 - 128 * j, 256 - 128 * j)
+            msend[h, j, half] = (mown[h, d, half] + mgot[h, j].astype(F32)).astype(BF)
+            msend[h, j, rest] = mown[h, d, rest].astype(BF)
+            send(msend.at[h, j], mrecv.at[h, j], mr_send.at[1], mr_recv.at[h, 1], along("x", d))
+
+    def mix_out(h):
+        bytes_of(mrecv.at[h], mr_recv.at[h, 1])
+        at = pl.ds(256 * h, 256)
+        out_a[256 * h : 256 * h + 256] = (mown[h, 0] + mrecv[h, 0].astype(F32) + mrecv[h, 1].astype(F32)).astype(BF)
+        pltpu.make_async_copy(out_a.at[at], far_a.at[at], out_sem.at[0]).start()
 
     def arrive(n):
         k = 2 * PER if n < NC - 1 else 2 * PER - 1
@@ -456,6 +480,12 @@
             i, cs = PER * n + b // 2, b % 2
             if i < 15:
                 to = ((z + HOPS[i]) % 16) * 2 + cs
+                if HOPS[i] == 8 and cs == 1:
+                    pltpu.make_async_remote_copy(
+                        src_ref=rows.at[2 * PER * n + b], dst_ref=rwait, send_sem=r_send, recv_sem=t_recv.at[1],
+                        device_id=(((z + 15) % 16) * 2 + c, t), device_id_type=MESH,
+                    ).start()
+                    continue
                 pltpu.make_async_remote_copy(
                     src_ref=rows.at[2 * PER * n + b], dst_ref=ret.at[e], send_sem=r_send, recv_sem=r_recv,
                     device_id=(to, t), device_id_type=MESH,
@@ -479,8 +509,9 @@
         arrive, relay, project, partial_sum, activate,
         lambda n: hid_steps[n][1](), lambda n: hid_steps[n][2](), lambda n: hid_steps[n][3](), finish,
         lambda n: pass_weights(), near_weights, lambda n: scan_prior(), lambda n: cell_out(),
-        lambda n: mix_relay(), lambda n: mix_part(), lambda n: mix_sum(), lambda n: mix_out(),
+        mix_relay, mix_part, mix_sum, mix_out,
         dispatch, lambda n: far_weights(), lambda n: weights_out(), lambda n: states(),
+        lambda n: onward_rows(), lambda n: onward_results(),
     ]
     for which, n in ORDER:
         stages[which](n)
@@ -488,10 +519,11 @@
 
     bytes_of(wt.at[pl.ds(0, 3)], w_send)
     bytes_of(wr, far_send)
+    bytes_of(xs.at[pl.ds(0, 2)], t_send)
     bytes_of(wm.at[pl.ds(0, 3)], mw_send)
     bytes_of(hid.at[:, 0, pl.ds(0, 3)], ag_near)
     bytes_of(hid.at[:, pl.ds(0, 3)], ag_wide)
-    bytes_of(mixed.at[pl.ds(0, 3)], ma_send)
+    bytes_of(mixed.at[:, pl.ds(0, 3)], ma_send)
     bytes_of(mfar, mr_send.at[0])
     bytes_of(msend, mr_send.at[1])
     bytes_of(xa.at[:, pl.ds(0, 3)], xg_send)
@@ -538,6 +570,8 @@
             pltpu.VMEM((2, 256), F32),
             pltpu.VMEM((512, 256), BF),
             pltpu.VMEM((256, 256), BF),
+            pltpu.VMEM((32, 256), BF),
+            pltpu.VMEM((32, 256), BF),
             pltpu.VMEM((4, 4, 256, 256), BF),
             pltpu.VMEM((2, 2, 256, 256), BF),
             pltpu.VMEM((1024, 256), BF),
@@ -554,12 +588,12 @@
             pltpu.VMEM((NC, 4, 4, 64, S), BF),
             pltpu.VMEM((32, 32, 256), BF),
             pltpu.VMEM((32, 32, 256), BF),
-            pltpu.VMEM((4, 512, 256), BF),
-            pltpu.VMEM((2, 256, 256), BF),
-            pltpu.VMEM((2, 256, 256), BF),
-            pltpu.VMEM((2, 512, 256), BF),
-            pltpu.VMEM((2, 512, 256), BF),
-            pltpu.VMEM((4, 512, 256), F32),
+            pltpu.VMEM((2, 4, 256, 256), BF),
+            pltpu.VMEM((2, 2, 128, 256), BF),
+            pltpu.VMEM((2, 2, 128, 256), BF),
+            pltpu.VMEM((2, 2, 256, 256), BF),
+            pltpu.VMEM((2, 2, 256, 256), BF),
+            pltpu.VMEM((2, 4, 256, 256), F32),
             pltpu.VMEM((32, 16, 128), BF),
             pltpu.VMEM((32, 16, 128), BF),
             pltpu.VMEM((32, 8, 128), BF),
@@ -586,9 +620,9 @@
             dma,
             dma,
             dma,
+            dma((2, 2)),
             dma((2,)),
-            dma((2,)),
-            dma((2,)),
+            dma((2, 2)),
             dma((2,)),
             dma((NC, 2)),
             dma,
@@ -596,6 +630,8 @@
             dma((NC, 4)),
             dma,
             dma,
+            dma,
+            dma((2,)),
         ],
         compiler_params=pltpu.CompilerParams(
             collective_id=0, has_side_effects=True, vmem_limit_bytes=56 * 1024 * 1024

time: 97.8 us -> 95.4 us (0.975)
  Pallas kernels: 97 us -> 94.6 us
    pallas_call x1, Pallas kernels: 95.2 us -> 92.9 us  [body(): pl.pallas_call(kernel, out_shape=(jax.ShapeDtypeStruct((512, 256), BF), j...]
where the time goes in v4:
time: 95.4 us; the launch traced here: 95.3 us
  Pallas kernels  94.6 us (99%)
    pallas_call x1, Pallas kernels, body(): pl.pallas_call(kernel, out_shape=(jax.ShapeDtypeStruct((512, 256), BF), j...  92.9 us

profile of v4, /device:TPU:1, one launch (start us, length us, event | category | flops | bytes accessed | tf_op | source)
XLA Modules:
  0.0 95.3 jit_solution(10676736941162376712)
XLA Ops:
  0.6 92.9 %shard_map.149 = (bf16[512,256]{1,0:T(8,128)(2,1)}, bf16[256,256]{1,0:T(8,128)(2,1)}) custom-call(bf16[512,128]{1,0:T(8,128)(2,1)} %q_hbm.1, bf16[512,128]{1,0:T(8,128)(2,1)} %k_hbm.1, bf16[512,256]{1,0:T(8,128)(2,1)} %v_hbm.1, f32[1,512]{1,0:T(1,128)} %ig_hbm.1, f32[1,512]{1,0:T(1,128)} %fg_hbm.1, bf16[512,256]{1,0:T(8,128)(2,1)} %og_hbm.1, ...), custom_call_target="tpu_custom_call" | custom-call | tf_op jit(solution)/shard_map/pallas_call | solution.py:555
  93.6 1.7 %shard_map.150 = (bf16[512,256]{1,0:T(8,128)(2,1)}, bf16[256,256]{1,0:T(8,128)(2,1)}) custom-call(bf16[512,256]{1,0:T(8,128)(2,1)} %get-tuple-element.4.a_in, bf16[256,256]{1,0:T(8,128)(2,1)} %get-tuple-element.5.b_in), custom_call_target="tpu_custom_call" | custom-call | tf_op jit(solution)/shard_map/pallas_call | solution.py:640
